TPU v7x, 32 devices: a whole 2x2x4 slice. The times are simulated.
32 devices in a mesh: sp: 8 (over z, y), tp: 4 (over x, core).
Axes of the slice: x: 2, y: 2, z: 4, core: 2. Of those that a mesh axis runs over, the one named last changes fastest.
Arguments:
- tokens: bfloat16 [4096, 2048], P(('sp', 'tp')), may hold values from -6 to 6
- input_gain: float32 [2048], replicated, may hold values from 0.1 to 1.9
- recur_query: bfloat16 [2048, 2048], P(None, 'tp'), may hold values from -0.125 to 0.125
- recur_forget: bfloat16 [2048, 2048], P(None, 'tp'), may hold values from -0.125 to 0.125
- recur_input: bfloat16 [2048, 1024], P(None, 'tp'), may hold values from -0.125 to 0.125
- recur_gate: bfloat16 [2048, 1024], P(None, 'tp'), may hold values from -0.125 to 0.125
- first_query: bfloat16 [2048, 512], P(None, 'tp'), may hold values from -0.18782524 to 0.18782524
- second_query: bfloat16 [2048, 512], P(None, 'tp'), may hold values from -0.18782524 to 0.18782524
- first_key: bfloat16 [2048, 512], P(None, 'tp'), may hold values from -5.7452426 to 5.7452426
- second_key: bfloat16 [2048, 512], P(None, 'tp'), may hold values from -5.7452426 to 5.7452426
- diff_value: bfloat16 [2048, 1024], P(None, 'tp'), may hold values from -0.125 to 0.125
- forget_floor: float32 [16, 128], P('tp'), may hold values from 9.765625e-05 to 0.08
- decay_shift: float32 [16, 4096], P('tp', 'sp'), may hold values from -0.7 to 0
- recur_gain: float32 [64], replicated, may hold values from 0.1 to 1.9
- diff_gain: float32 [64], replicated, may hold values from 0.1 to 1.9
- diff_lambda: float32 [16], P('tp'), may hold values from 0.3 to 0.8
- recur_out: bfloat16 [1024, 2048], P('tp'), may hold values from -0.125 to 0.125
- diff_out: bfloat16 [1024, 2048], P('tp'), may hold values from -0.125 to 0.125
- final_gain: float32 [2048], replicated, may hold values from 0.1 to 1.9
Outputs:
- layer_out: bfloat16 [4096, 2048], P(('sp', 'tp'))
- row_logsum: float32 [2, 16, 4096], P(None, 'tp', 'sp')
All inputs are finite; a program needn't handle non-finite values.
Results may differ from a plain program's by a relative error of at most 0.014.
Values may be sent and summed in bfloat16 or wider, within the bound.
A program may use at most 128 MiB of HBM per device.

v0:
```python
import math

import jax
import jax.numpy as jnp
from jax import lax
from jax.sharding import PartitionSpec as P

SPAN = 64


EPSILON = 1e-06
TOP_PRECISION = lax.Precision.HIGHEST
NEGATIVE = -1e30


def entering(x, axis, join, neutral):
    place = lax.axis_index(axis)
    gathered = jax.tree.map(
        lambda a, kind: lax.all_gather(a.astype(kind), axis), x, (jnp.bfloat16, jnp.bfloat16)
    )
    state = jax.tree.map(lambda a, e: jnp.zeros_like(a) + jnp.asarray(e, a.dtype), x, neutral)

    def one(turn, state):
        return join(
            state,
            jax.tree.map(
                lambda a, own: lax.dynamic_index_in_dim(a, turn, 0, False).astype(own.dtype),
                gathered,
                x,
            ),
        )

    return lax.fori_loop(0, place, one, state)


def row_norm(value_rows, gain):
    mean_square = jnp.mean(value_rows * value_rows, axis=-1, keepdims=True)
    return value_rows * lax.rsqrt(mean_square + EPSILON) * gain


def block_step(memory_state, inputs):
    query_vector, keyed_values, value_rows, decay = inputs
    length = query_vector.shape[1]
    running_total = jnp.cumsum(decay, axis=1)
    causal = jnp.tril(jnp.ones((length, length), bool))
    carried_state = jnp.einsum(
        "sqr,sri->sqi", query_vector * jnp.exp(running_total), memory_state, precision=TOP_PRECISION
    )
    spread = running_total[:, :, None, :] - running_total[:, None, :, :]
    factors = jnp.exp(jnp.where(causal[None, :, :, None], spread, -jnp.inf))
    scores = jnp.einsum(
        "htk,htsk,hsk->hts", query_vector, factors, keyed_values, precision=TOP_PRECISION
    )
    within = jnp.einsum("hts,hsv->htv", scores, value_rows, precision=TOP_PRECISION)
    final_state = running_total[:, -1]
    memory_state = jnp.exp(final_state)[:, :, None] * memory_state + jnp.einsum(
        "ojr,ojw->orw",
        keyed_values * jnp.exp(final_state[:, None] - running_total),
        value_rows,
        precision=TOP_PRECISION,
    )
    return (memory_state, carried_state + within)


def local_recurrence(query_vector, keyed_values, value_rows, decay):
    total = query_vector.shape[0]
    heads = query_vector.shape[1]
    blocks = total // SPAN

    def arrange(array):
        return jnp.transpose(array.reshape(blocks, SPAN, heads, array.shape[-1]), (0, 2, 1, 3))

    memory_state = jnp.zeros((heads, query_vector.shape[2], value_rows.shape[2]), jnp.float32)
    memory_state, outputs = lax.scan(
        block_step,
        memory_state,
        (arrange(query_vector), arrange(keyed_values), arrange(value_rows), arrange(decay)),
    )
    return (
        jnp.transpose(outputs, (0, 2, 1, 3)).reshape(total, heads, value_rows.shape[2]),
        memory_state,
    )


def body(
    tokens,
    input_gain,
    recur_query,
    recur_forget,
    recur_input,
    recur_gate,
    first_query,
    second_query,
    first_key,
    second_key,
    diff_value,
    forget_floor,
    decay_shift,
    recur_gain,
    diff_gain,
    diff_lambda,
    recur_out,
    diff_out,
    final_gain,
):
    groups = lax.axis_size("tp")
    position = lax.axis_index("sp")
    normed = row_norm(tokens.astype(jnp.float32), input_gain).astype(jnp.bfloat16)
    joined = jnp.concatenate(
        [
            recur_query,
            recur_forget,
            recur_input,
            recur_gate,
            first_query,
            second_query,
            first_key,
            second_key,
            diff_value,
        ],
        axis=1,
    )
    projected = jnp.dot(
        lax.all_gather(normed, "tp", axis=0, tiled=True), joined, preferred_element_type=jnp.float32
    ).astype(jnp.bfloat16)
    rows = projected.shape[0]
    heads = diff_lambda.shape[0]
    state_width = forget_floor.shape[1]
    head_width = recur_gain.shape[0]
    pair_width = first_query.shape[1] // heads
    wide = heads * state_width
    narrow = heads * head_width
    small = heads * pair_width
    base = 2 * wide + 2 * narrow
    query_readout = projected[:, :wide].astype(jnp.float32).reshape(rows, heads, state_width)
    forget_logit = (
        projected[:, wide : 2 * wide].astype(jnp.float32).reshape(rows, heads, state_width)
    )
    input_rows = (
        projected[:, 2 * wide : 2 * wide + narrow]
        .astype(jnp.float32)
        .reshape(rows, heads, head_width)
    )
    gate_rows = projected[:, 2 * wide + narrow : base].astype(jnp.float32)
    query_one = projected[:, base : base + small].reshape(rows, heads, pair_width)
    query_two = projected[:, base + small : base + 2 * small].reshape(rows, heads, pair_width)
    keys_values = projected[:, base + 2 * small :]
    keyed_values = forget_floor[None] * jax.nn.sigmoid(-forget_logit)
    decay = jnp.log1p(-keyed_values) + jnp.transpose(decay_shift)[:, :, None]
    local_out, local_state = local_recurrence(query_readout, keyed_values, input_rows, decay)
    running_state = jnp.cumsum(decay, axis=0)
    block_total = running_state[-1]

    def combine(earlier, later):
        return (earlier[0] + later[0], jnp.exp(later[0])[:, :, None] * earlier[1] + later[1])

    incoming_state = entering(
        (block_total, local_state),
        "sp",
        combine,
        (jnp.zeros_like(block_total), jnp.zeros_like(local_state)),
    )[1]
    recurrent = local_out + jnp.einsum(
        "oiz,izx->oix",
        query_readout * jnp.exp(running_state),
        incoming_state,
        precision=TOP_PRECISION,
    )
    recur_mix = row_norm(recurrent, recur_gain).reshape(rows, narrow) * jax.nn.silu(gate_rows)
    query_start = position * rows
    query_place = query_start + jnp.arange(rows)
    scale = pair_width ** (-0.5)
    queries = jnp.stack([query_one, query_two])
    initial = (
        jnp.full((2, heads, rows), NEGATIVE, jnp.float32),
        jnp.zeros((2, heads, rows), jnp.float32),
        jnp.zeros((2, heads, rows, head_width), jnp.float32),
    )
    carry = initial
    piece = lax.all_gather(keys_values, "sp", axis=0, tiled=True)
    count = piece.shape[0]
    step = math.gcd(count, 512)

    def one_block(index, carry):
        block = lax.dynamic_slice_in_dim(piece, index * step, step, 0)
        key_start = index * step

        def update(carry):
            maxima, sums, totals = carry
            keys = jnp.stack(
                [
                    block[:, :small].reshape(step, heads, pair_width),
                    block[:, small : 2 * small].reshape(step, heads, pair_width),
                ]
            )
            value_rows = block[:, 2 * small :].reshape(step, heads, head_width)
            scores = (
                jnp.einsum("jqhe,jkhe->jhqk", queries, keys, preferred_element_type=jnp.float32)
                * scale
            )
            visible = query_place[:, None] >= (key_start + jnp.arange(step))[None, :]
            scores = jnp.where(visible, scores, NEGATIVE)
            newest = jnp.maximum(maxima, jnp.max(scores, axis=-1))
            weights = jnp.where(visible, jnp.exp(scores - newest[..., None]), 0.0)
            shrink = jnp.exp(maxima - newest)
            sums = sums * shrink + jnp.sum(weights, axis=-1)
            totals = totals * shrink[..., None] + jnp.einsum(
                "jhqk,khe->jhqe",
                weights.astype(jnp.bfloat16),
                value_rows,
                preferred_element_type=jnp.float32,
            )
            return (newest, sums, totals)

        return lax.cond(
            key_start <= query_start + rows - 1, update, lambda unchanged: unchanged, carry
        )

    maxima, sums, totals = lax.fori_loop(0, count // step, one_block, carry)
    row_logsum = maxima + jnp.log(sums)
    combined = (
        totals[0] / sums[0][..., None] - diff_lambda[:, None, None] * totals[1] / sums[1][..., None]
    )
    diff_mix = jnp.transpose(row_norm(combined, diff_gain), (1, 0, 2)).reshape(rows, narrow)
    mixed = jnp.concatenate([recur_mix, diff_mix], axis=1).astype(jnp.bfloat16)
    full_recur, full_diff = (
        lax.all_gather(recur_out, "tp", axis=0, tiled=True),
        lax.all_gather(diff_out, "tp", axis=0, tiled=True),
    )
    width = full_recur.shape[1]
    full = jnp.stack(
        [full_recur.reshape(groups, narrow, width), full_diff.reshape(groups, narrow, width)],
        axis=1,
    ).reshape(2 * groups * narrow, width)
    moved = lax.all_to_all(mixed, "tp", split_axis=0, concat_axis=1, tiled=True)
    merged = jnp.dot(moved, full, preferred_element_type=jnp.float32)
    layer_out = row_norm(merged, final_gain).astype(jnp.bfloat16)
    return (layer_out, row_logsum)


def solution(mesh):
    in_specs = (
        P(("sp", "tp"), None),
        P(),
        P(None, "tp"),
        P(None, "tp"),
        P(None, "tp"),
        P(None, "tp"),
        P(None, "tp"),
        P(None, "tp"),
        P(None, "tp"),
        P(None, "tp"),
        P(None, "tp"),
        P("tp", None),
        P("tp", "sp"),
        P(),
        P(),
        P("tp"),
        P("tp", None),
        P("tp", None),
        P(),
    )
    out_specs = (P(("sp", "tp"), None), P(None, "tp", "sp"))
    return jax.shard_map(body, mesh=mesh, in_specs=in_specs, out_specs=out_specs, check_vma=False)
```

profile of v0, /device:TPU:31, one launch (start us, length us, event | category | flops | bytes accessed | tf_op | source)
XLA Modules:
  0.0 413.7 jit_solution(18305595248429538303)
XLA Ops:
  8.6 2.0 fusion.51
  10.8 3.3 constant_dynamic-update-slice_fusion.8
  14.1 3.1 constant_dynamic-update-slice_fusion.7
  24.2 9.6 %all-gather.6.cloned.1.call-done = bf16[512,2048]{1,0:T(8,128)(2,1)} async-done(((bf16[128,2048]{1,0:T(8,128)(2,1)}), bf16[512,2048]{1,0:T(8,128)(2,1)}) %all-gather.6.cloned.1.call-update) | async-done | bytes 2097168 | tf_op jit(solution)/shard_map/all_gather | solution.py:124
  33.8 9.3 %convolution_convert_fusion = bf16[512,2304]{1,0:T(8,128)(2,1)S(1)} fusion(bf16[512,2048]{1,0:T(8,128)(2,1)} %all-gather.6.cloned.1.call-done, bf16[2048,2304]{1,0:T(8,128)(2,1)} %constant_dynamic-update-slice_fusion), kind=kOutput, calls=%fused_computation.62 | convolution fusion | flops 4833017856 | bytes 13893632 | tf_op jit(solution)/shard_map/dot_general | solution.py:123
  47.0 2.4 fusion.69
  49.4 1.8 slice_convert_fusion.1
  55.7 3.5 fusion.58
  59.2 166.9 %while.47 = (s32[]{:T(128)}, f32[4,128,64]{1,2,0:T(8,128)S(1)}, f32[8,4,64,64]{3,2,1,0:T(8,128)}, f32[8,4,64,128]{3,2,1,0:T(8,128)}, f32[8,4,64,128]{3,2,1,0:T(8...) while((s32[]{:T(128)}, f32[4,128,64]{1,2,0:T(8,128)S(1)}, ...), condition=%wide.region_3.4_spmd.clone, body=%wide.region_1.3_spmd.clone.sunk | while | flops 96686080 | bytes 3168380 | solution.py:74
  61.8 15.6 %fusion.100 = f32[4,64,1,64]{3,2,1,0:T(1,128)} fusion(f32[4,64,128,1]{2,3,1,0:T(1,128)S(1)} %bitcast.182, f32[4,64,128]{2,1,0:T(8,128)} %get-tuple-element.685, f32[4,64,128]{2,1,0:T(8,128)S(1)} %reduce_window_sum.32, pred[64,64]{1,0:T(8,128)(4,1)S(1)} %iota_compare_fusion.2), kind=kOutput, calls=%fused_computation.24.clone.1 | convolution fusion | flops 31457280 | bytes 462848 | tf_op jit(solution)/shard_map/while/body/eval_jaxpr/htk,htsk,hsk->hts/dot_general | solution.py:51
  77.7 1.9 fusion.101
  80.0 1.6 dynamic-slice_bitcast_fusion.4
  82.7 15.6 %fusion.100 = f32[4,64,1,64]{3,2,1,0:T(1,128)} fusion(f32[4,64,128,1]{2,3,1,0:T(1,128)S(1)} %bitcast.182, f32[4,64,128]{2,1,0:T(8,128)} %get-tuple-element.685, f32[4,64,128]{2,1,0:T(8,128)S(1)} %reduce_window_sum.32, pred[64,64]{1,0:T(8,128)(4,1)S(1)} %iota_compare_fusion.2), kind=kOutput, calls=%fused_computation.24.clone.1 | convolution fusion | flops 31457280 | bytes 462848 | tf_op jit(solution)/shard_map/while/body/eval_jaxpr/htk,htsk,hsk->hts/dot_general | solution.py:51
  98.6 1.9 fusion.101
  103.5 15.6 %fusion.100 = f32[4,64,1,64]{3,2,1,0:T(1,128)} fusion(f32[4,64,128,1]{2,3,1,0:T(1,128)S(1)} %bitcast.182, f32[4,64,128]{2,1,0:T(8,128)} %get-tuple-element.685, f32[4,64,128]{2,1,0:T(8,128)S(1)} %reduce_window_sum.32, pred[64,64]{1,0:T(8,128)(4,1)S(1)} %iota_compare_fusion.2), kind=kOutput, calls=%fused_computation.24.clone.1 | convolution fusion | flops 31457280 | bytes 462848 | tf_op jit(solution)/shard_map/while/body/eval_jaxpr/htk,htsk,hsk->hts/dot_general | solution.py:51
  119.4 1.9 fusion.101
  124.3 15.6 %fusion.100 = f32[4,64,1,64]{3,2,1,0:T(1,128)} fusion(f32[4,64,128,1]{2,3,1,0:T(1,128)S(1)} %bitcast.182, f32[4,64,128]{2,1,0:T(8,128)} %get-tuple-element.685, f32[4,64,128]{2,1,0:T(8,128)S(1)} %reduce_window_sum.32, pred[64,64]{1,0:T(8,128)(4,1)S(1)} %iota_compare_fusion.2), kind=kOutput, calls=%fused_computation.24.clone.1 | convolution fusion | flops 31457280 | bytes 462848 | tf_op jit(solution)/shard_map/while/body/eval_jaxpr/htk,htsk,hsk->hts/dot_general | solution.py:51
  140.2 1.9 fusion.101
  145.1 15.6 %fusion.100 = f32[4,64,1,64]{3,2,1,0:T(1,128)} fusion(f32[4,64,128,1]{2,3,1,0:T(1,128)S(1)} %bitcast.182, f32[4,64,128]{2,1,0:T(8,128)} %get-tuple-element.685, f32[4,64,128]{2,1,0:T(8,128)S(1)} %reduce_window_sum.32, pred[64,64]{1,0:T(8,128)(4,1)S(1)} %iota_compare_fusion.2), kind=kOutput, calls=%fused_computation.24.clone.1 | convolution fusion | flops 31457280 | bytes 462848 | tf_op jit(solution)/shard_map/while/body/eval_jaxpr/htk,htsk,hsk->hts/dot_general | solution.py:51
  161.1 1.9 fusion.101
  166.0 15.6 %fusion.100 = f32[4,64,1,64]{3,2,1,0:T(1,128)} fusion(f32[4,64,128,1]{2,3,1,0:T(1,128)S(1)} %bitcast.182, f32[4,64,128]{2,1,0:T(8,128)} %get-tuple-element.685, f32[4,64,128]{2,1,0:T(8,128)S(1)} %reduce_window_sum.32, pred[64,64]{1,0:T(8,128)(4,1)S(1)} %iota_compare_fusion.2), kind=kOutput, calls=%fused_computation.24.clone.1 | convolution fusion | flops 31457280 | bytes 462848 | tf_op jit(solution)/shard_map/while/body/eval_jaxpr/htk,htsk,hsk->hts/dot_general | solution.py:51
  181.9 1.9 fusion.101
  186.8 15.6 %fusion.100 = f32[4,64,1,64]{3,2,1,0:T(1,128)} fusion(f32[4,64,128,1]{2,3,1,0:T(1,128)S(1)} %bitcast.182, f32[4,64,128]{2,1,0:T(8,128)} %get-tuple-element.685, f32[4,64,128]{2,1,0:T(8,128)S(1)} %reduce_window_sum.32, pred[64,64]{1,0:T(8,128)(4,1)S(1)} %iota_compare_fusion.2), kind=kOutput, calls=%fused_computation.24.clone.1 | convolution fusion | flops 31457280 | bytes 462848 | tf_op jit(solution)/shard_map/while/body/eval_jaxpr/htk,htsk,hsk->hts/dot_general | solution.py:51
  202.8 1.9 fusion.101
  207.7 15.6 %fusion.100 = f32[4,64,1,64]{3,2,1,0:T(1,128)} fusion(f32[4,64,128,1]{2,3,1,0:T(1,128)S(1)} %bitcast.182, f32[4,64,128]{2,1,0:T(8,128)} %get-tuple-element.685, f32[4,64,128]{2,1,0:T(8,128)S(1)} %reduce_window_sum.32, pred[64,64]{1,0:T(8,128)(4,1)S(1)} %iota_compare_fusion.2), kind=kOutput, calls=%fused_computation.24.clone.1 | convolution fusion | flops 31457280 | bytes 462848 | tf_op jit(solution)/shard_map/while/body/eval_jaxpr/htk,htsk,hsk->hts/dot_general | solution.py:51
  223.6 1.9 fusion.101
  226.1 1.7 fusion.55
  232.3 12.6 %all_gather.23 = bf16[8,4,128]{2,1,0:T(4,128)(2,1)S(1)} all-gather(bf16[1,4,128]{2,1,0:T(4,128)(2,1)S(1)} %copy.95), channel_id=1, replica_groups=mesh['sp'=8,'tp'=4] {'sp'}, dimensions={0}, use_global_device_ids=true | all-gather | bytes 9216 | tf_op jit(solution)/shard_map/all_gather | solution.py:19
  244.9 27.6 %all-gather = bf16[32,128,64]{1,2,0:T(8,128)(2,1)} all-gather(bf16[4,128,64]{1,2,0:T(8,128)(2,1)S(1)} %convert_element_type.64), channel_id=2, replica_groups=mesh['sp'=8,'tp'=4] {'sp'}, dimensions={0}, use_global_device_ids=true | all-gather | bytes 589824 | tf_op jit(solution)/shard_map/all_gather | solution.py:19
  272.6 8.4 %while.45 = (s32[]{:T(128)}, f32[4,128,64]{2,1,0:T(8,128)S(1)}, s32[]{:T(128)}, bf16[8,4,128]{2,1,0:T(4,128)(2,1)S(1)}, bf16[8,4,128,64]{2,3,1,0:T(8,128)(2,1)}, /*index=5*/s32[]{:T(128)}, s32[]{:T(128)}, s32[]{:T(128)}) while((s32[]{:T(128)}, f32[4,128,64]{2,1,0:T(8,128)S(1)}, s32[]{:T(128)}, bf16[8,4,128]{2,1,0:T(4,128)(2,1)S(1)}, ...), condition=%wide.region_7.8_spmd, body=%wide.region_6.7_spmd.sunk | while | flops 98821 | bytes 595071 | solution.py:33
  285.2 6.4 %copy.103 = bf16[4096,512]{0,1:T(8,128)(2,1)} copy(bf16[4096,512]{1,0:T(8,128)(2,1)} %all-gather.8.cloned.1.call-done) | data formatting | bytes 8388608
  291.8 85.6 %while.46 = (s32[]{:T(128)}, f32[2,4,512]{2,1,0:T(4,128)S(1)}, f32[2,4,512]{2,1,0:T(4,128)S(1)}, f32[2,4,512,64]{2,3,0,1:T(8,128)S(1)}, s32[]{:T(128)}, /*index=...) while((s32[]{:T(128)}, f32[2,4,512]{2,1,0:T(4,128)S(1)}, ...), condition=%wide.region_14.15_spmd.clone, body=%wide.region_9.14_spmd.clone.sunk | while | flops 422454272 | bytes 30175556 | solution.py:219
  291.8 10.7 %conditional.3 = ((f32[2,4,512]{2,1,0:T(4,128)S(1)}, f32[2,4,512]{2,1,0:T(4,128)S(1)}, f32[2,4,512,64]{2,3,0,1:T(8,128)S(1)})) conditional(s32[]{:T(128)} %convert_element_type.105, (f32[2,4,512]{2,1,0:T(4,128)S(1)}, f32[2,4,512]{2,1,0:T(4,128)S(1)}, f32[2,4,512,64]{2,3,0,1:T(8,128)S(1)}) %tuple.119, (s32[]{:T(128)}, s32[]{:T(128)}, ...), branch_computations={%region_10.10_spmd, %region_11.13_spmd} | conditional | flops 422454272 | bytes 30173294 | solution.py:215
  294.7 3.6 fusion.3
  299.3 3.1 fusion.10
  302.5 10.7 %conditional.3 = ((f32[2,4,512]{2,1,0:T(4,128)S(1)}, f32[2,4,512]{2,1,0:T(4,128)S(1)}, f32[2,4,512,64]{2,3,0,1:T(8,128)S(1)})) conditional(s32[]{:T(128)} %convert_element_type.105, (f32[2,4,512]{2,1,0:T(4,128)S(1)}, f32[2,4,512]{2,1,0:T(4,128)S(1)}, f32[2,4,512,64]{2,3,0,1:T(8,128)S(1)}) %tuple.119, (s32[]{:T(128)}, s32[]{:T(128)}, ...), branch_computations={%region_10.10_spmd, %region_11.13_spmd} | conditional | flops 422454272 | bytes 30173294 | solution.py:215
  303.7 1.6 fusion.2
  305.4 3.6 fusion.3
  310.0 3.1 fusion.10
  313.2 10.7 %conditional.3 = ((f32[2,4,512]{2,1,0:T(4,128)S(1)}, f32[2,4,512]{2,1,0:T(4,128)S(1)}, f32[2,4,512,64]{2,3,0,1:T(8,128)S(1)})) conditional(s32[]{:T(128)} %convert_element_type.105, (f32[2,4,512]{2,1,0:T(4,128)S(1)}, f32[2,4,512]{2,1,0:T(4,128)S(1)}, f32[2,4,512,64]{2,3,0,1:T(8,128)S(1)}) %tuple.119, (s32[]{:T(128)}, s32[]{:T(128)}, ...), branch_computations={%region_10.10_spmd, %region_11.13_spmd} | conditional | flops 422454272 | bytes 30173294 | solution.py:215
  314.4 1.6 fusion.2
  316.1 3.6 fusion.3
  320.7 3.1 fusion.10
  323.9 10.7 %conditional.3 = ((f32[2,4,512]{2,1,0:T(4,128)S(1)}, f32[2,4,512]{2,1,0:T(4,128)S(1)}, f32[2,4,512,64]{2,3,0,1:T(8,128)S(1)})) conditional(s32[]{:T(128)} %convert_element_type.105, (f32[2,4,512]{2,1,0:T(4,128)S(1)}, f32[2,4,512]{2,1,0:T(4,128)S(1)}, f32[2,4,512,64]{2,3,0,1:T(8,128)S(1)}) %tuple.119, (s32[]{:T(128)}, s32[]{:T(128)}, ...), branch_computations={%region_10.10_spmd, %region_11.13_spmd} | conditional | flops 422454272 | bytes 30173294 | solution.py:215
  326.8 3.6 fusion.3
  331.4 3.1 fusion.10
  334.6 10.7 %conditional.3 = ((f32[2,4,512]{2,1,0:T(4,128)S(1)}, f32[2,4,512]{2,1,0:T(4,128)S(1)}, f32[2,4,512,64]{2,3,0,1:T(8,128)S(1)})) conditional(s32[]{:T(128)} %convert_element_type.105, (f32[2,4,512]{2,1,0:T(4,128)S(1)}, f32[2,4,512]{2,1,0:T(4,128)S(1)}, f32[2,4,512,64]{2,3,0,1:T(8,128)S(1)}) %tuple.119, (s32[]{:T(128)}, s32[]{:T(128)}, ...), branch_computations={%region_10.10_spmd, %region_11.13_spmd} | conditional | flops 422454272 | bytes 30173294 | solution.py:215
  335.9 1.6 fusion.2
  337.5 3.6 fusion.3
  342.1 3.1 fusion.10
  345.3 10.7 %conditional.3 = ((f32[2,4,512]{2,1,0:T(4,128)S(1)}, f32[2,4,512]{2,1,0:T(4,128)S(1)}, f32[2,4,512,64]{2,3,0,1:T(8,128)S(1)})) conditional(s32[]{:T(128)} %convert_element_type.105, (f32[2,4,512]{2,1,0:T(4,128)S(1)}, f32[2,4,512]{2,1,0:T(4,128)S(1)}, f32[2,4,512,64]{2,3,0,1:T(8,128)S(1)}) %tuple.119, (s32[]{:T(128)}, s32[]{:T(128)}, ...), branch_computations={%region_10.10_spmd, %region_11.13_spmd} | conditional | flops 422454272 | bytes 30173294 | solution.py:215
  346.6 1.6 fusion.2
  348.2 3.6 fusion.3
  352.8 3.1 fusion.10
  356.0 10.7 %conditional.3 = ((f32[2,4,512]{2,1,0:T(4,128)S(1)}, f32[2,4,512]{2,1,0:T(4,128)S(1)}, f32[2,4,512,64]{2,3,0,1:T(8,128)S(1)})) conditional(s32[]{:T(128)} %convert_element_type.105, (f32[2,4,512]{2,1,0:T(4,128)S(1)}, f32[2,4,512]{2,1,0:T(4,128)S(1)}, f32[2,4,512,64]{2,3,0,1:T(8,128)S(1)}) %tuple.119, (s32[]{:T(128)}, s32[]{:T(128)}, ...), branch_computations={%region_10.10_spmd, %region_11.13_spmd} | conditional | flops 422454272 | bytes 30173294 | solution.py:215
  357.3 1.6 fusion.2
  358.9 3.6 fusion.3
  363.5 3.1 fusion.10
  366.7 10.7 %conditional.3 = ((f32[2,4,512]{2,1,0:T(4,128)S(1)}, f32[2,4,512]{2,1,0:T(4,128)S(1)}, f32[2,4,512,64]{2,3,0,1:T(8,128)S(1)})) conditional(s32[]{:T(128)} %convert_element_type.105, (f32[2,4,512]{2,1,0:T(4,128)S(1)}, f32[2,4,512]{2,1,0:T(4,128)S(1)}, f32[2,4,512,64]{2,3,0,1:T(8,128)S(1)}) %tuple.119, (s32[]{:T(128)}, s32[]{:T(128)}, ...), branch_computations={%region_10.10_spmd, %region_11.13_spmd} | conditional | flops 422454272 | bytes 30173294 | solution.py:215
  369.6 3.6 fusion.3
  374.2 3.1 fusion.10
  379.0 14.4 %all-to-all-start = ((bf16[4,128,512]{1,2,0:T(8,128)(2,1)}), bf16[4,128,512]{1,2,0:T(8,128)(2,1)S(1)}, u32[]{:S(2)}, u32[]{:S(2)}) async-start(bf16[4,128,512]{1,2,0:T(8,128)(2,1)} %copy.106), calls=%async_computation | async-start | bytes 1048576 | tf_op jit(solution)/shard_map/all_to_all | solution.py:235
  393.4 7.4 %pad_maximum_fusion = bf16[4,2,256,2048]{3,2,1,0:T(8,128)(2,1)} fusion(bf16[4,1,256,2048]{3,2,1,0:T(8,128)(2,1)} %bitcast.188, bf16[4,1,256,2048]{3,2,1,0:T(8,128)(2,1)} %bitcast.187), kind=kLoop, calls=%fused_computation.61 | loop fusion | flops 4194304 | bytes 16777216 | tf_op jit(solution)/shard_map/stack | solution.py:231
  401.5 4.7 %multiply_reduce_fusion = (f32[128]{0:T(128)S(1)}, f32[128,2048]{1,0:T(8,128)S(1)}) fusion(bf16[128,2048]{0,1:T(8,128)(2,1)S(1)} %bitcast.189, bf16[2048,2048]{1,0:T(8,128)(2,1)} %bitcast.180), kind=kOutput, calls=%fused_computation.81 | convolution fusion | flops 1074265984 | bytes 9961984 | tf_op jit(solution)/shard_map/dot_general | solution.py:236
  (262 shorter events, 84.5 us)
Async XLA Ops:
  7.2 10.0 %copy-start.1 = (bf16[2048,256]{1,0:T(8,128)(2,1)S(1)}, bf16[2048,256]{1,0:T(8,128)(2,1)}, u32[]{:S(2)}) copy-start(bf16[2048,256]{1,0:T(8,128)(2,1)} %param.31) | copy-start | bytes 3145732
  7.2 11.2 %copy-start.2 = (bf16[2048,256]{1,0:T(8,128)(2,1)S(1)}, bf16[2048,256]{1,0:T(8,128)(2,1)}, u32[]{:S(2)}) copy-start(bf16[2048,256]{1,0:T(8,128)(2,1)} %param.32) | copy-start | bytes 3145732
  7.2 26.6 %all-gather.6.cloned.1.call-start = ((), (), s32[]{:S(2)}) async-start(), calls=%async_computation.1 | async-start | bytes 2621440 | tf_op jit(solution)/shard_map/all_gather | solution.py:124
  10.7 12.4 %copy-start.3 = (bf16[2048,256]{1,0:T(8,128)(2,1)S(1)}, bf16[2048,256]{1,0:T(8,128)(2,1)}, u32[]{:S(2)}) copy-start(bf16[2048,256]{1,0:T(8,128)(2,1)} %param.37) | copy-start | bytes 3145732
  10.7 274.5 %all-gather.8.cloned.1.call-start = ((), (), s32[]{:S(2)}) async-start(), calls=%async_computation.2 | async-start | bytes 4718592 | tf_op jit(solution)/shard_map/all_gather | solution.py:180
  10.7 8.8 %copy-start.5 = (bf16[2048,128]{1,0:T(8,128)(2,1)S(1)}, bf16[2048,128]{1,0:T(8,128)(2,1)}, u32[]{:S(2)}) copy-start(bf16[2048,128]{1,0:T(8,128)(2,1)} %param.33) | copy-start | bytes 1572868
  10.7 9.6 %copy-start.6 = (bf16[2048,128]{1,0:T(8,128)(2,1)S(1)}, bf16[2048,128]{1,0:T(8,128)(2,1)}, u32[]{:S(2)}) copy-start(bf16[2048,128]{1,0:T(8,128)(2,1)} %param.34) | copy-start | bytes 1572868
  10.7 10.5 %copy-start.7 = (bf16[2048,128]{1,0:T(8,128)(2,1)S(1)}, bf16[2048,128]{1,0:T(8,128)(2,1)}, u32[]{:S(2)}) copy-start(bf16[2048,128]{1,0:T(8,128)(2,1)} %param.35) | copy-start | bytes 1572868
  10.8 11.4 %copy-start.8 = (bf16[2048,128]{1,0:T(8,128)(2,1)S(1)}, bf16[2048,128]{1,0:T(8,128)(2,1)}, u32[]{:S(2)}) copy-start(bf16[2048,128]{1,0:T(8,128)(2,1)} %param.36) | copy-start | bytes 1572868
  24.2 22.7 %copy-start.9 = (f32[4,512]{1,0:T(4,128)S(1)}, f32[4,512]{1,0:T(4,128)}, u32[]{:S(2)}) copy-start(f32[4,512]{1,0:T(4,128)} %param.39) | copy-start | bytes 24580
  43.0 1.4 copy-start
  44.4 11.2 %copy-start.11 = (f32[4,128]{1,0:T(4,128)S(1)}, f32[4,128]{1,0:T(4,128)}, u32[]{:S(2)}) copy-start(f32[4,128]{1,0:T(4,128)} %param.38) | copy-start | bytes 6148
  45.6 347.9 %all-gather.10.cloned.1.call-start = ((), (), s32[]{:S(2)}) async-start(), calls=%async_computation.3 | async-start | bytes 5242880 | tf_op jit(solution)/shard_map/all_gather | solution.py:227
  46.3 347.1 %all-gather.12.cloned.1.call-start = ((), (), s32[]{:S(2)}) async-start(), calls=%async_computation.4 | async-start | bytes 5242880 | tf_op jit(solution)/shard_map/all_gather | solution.py:228
  226.0 4.0 copy-start.4
  229.9 52.4 %copy-start.12 = (f32[64]{0:T(128)S(1)}, f32[64]{0:T(128)}, u32[]{:S(2)}) copy-start(f32[64]{0:T(128)} %param.40) | copy-start | bytes 772
  291.7 85.7 %copy-start.13 = (f32[4]{0:T(128)S(1)}, f32[4]{0:T(128)}, u32[]{:S(2)}) copy-start(f32[4]{0:T(128)} %param.42) | copy-start | bytes 52
  291.7 85.9 %copy-start.14 = (f32[64]{0:T(128)S(1)}, f32[64]{0:T(128)}, u32[]{:S(2)}) copy-start(f32[64]{0:T(128)} %param.41) | copy-start | bytes 772
  379.0 22.4 %all-to-all-start = ((bf16[4,128,512]{1,2,0:T(8,128)(2,1)}), bf16[4,128,512]{1,2,0:T(8,128)(2,1)S(1)}, u32[]{:S(2)}, u32[]{:S(2)}) async-start(bf16[4,128,512]{1,2,0:T(8,128)(2,1)} %copy.106), calls=%async_computation | async-start | bytes 1048576 | tf_op jit(solution)/shard_map/all_to_all | solution.py:235
  400.9 5.4 %copy-start.10 = (f32[2048]{0:T(1024)S(1)}, f32[2048]{0:T(1024)}, u32[]{:S(2)}) copy-start(f32[2048]{0:T(1024)} %param.45) | copy-start | bytes 24580
Sparse Core Ops, SparseCore 0:
  10.8 22.9 all-gather.5
  45.7 70.8 all-gather.7
  118.2 34.8 all-gather.9
  154.5 34.4 all-gather.11
where the time goes:
time: 416 us; the launch traced here: 414 us
  matrix products  198 us (48%)
  local copies, waits for them, and re-layouts  73.7 us (18%)
  other arithmetic  60.2 us (14%)
  blocking collectives  40.2 us (10%)
  starting transfers between devices  14.5 us (3%)
  between operations  14.2 us (3%)
  waiting for transfers between devices  10.9 us (3%)
    dot_general x8, matrix products, block_step(): jnp.einsum('htk,htsk,hsk->hts', query_vector, factors, keyed_values, prec...  125 us
    all_gather x2, blocking collectives, entering(): lax.all_gather(a.astype(kind), axis)  40.2 us
    convert_element_type x8, other arithmetic, update(): weights.astype(jnp.bfloat16)  28.9 us
    dot_general x8, matrix products, update(): jnp.einsum('jhqk,khe->jhqe', weights.astype(jnp.bfloat16), value_rows, pr...  24.9 us
    unnamed x39, local copies, waits for them, and re-layouts  20.1 us
    dot_general x8, matrix products, block_step(): jnp.einsum('hts,hsv->htv', scores, value_rows, precision=TOP_PRECISION)  15.2 us
    all_to_all x1, starting transfers between devices, body(): moved = lax.all_to_all(mixed, 'tp', split_axis=0, concat_axis=1, tiled=True)  14.4 us
    dot_general x8, matrix products, update(): jnp.einsum('jqhe,jkhe->jhqk', queries, keys, preferred_element_type=jnp.f...  13.1 us
  transfers between devices with their start and end apart: 5, of which 1 were waited for; matrix products, arithmetic and copies ran while one was open for 75% of the time, Pallas kernels for 0%

commit v1 on v0

v1 whole, which is shorter than its diff:
```python
import functools
import math

import jax
import jax.numpy as jnp
from jax import lax
from jax.experimental import pallas as pl
from jax.experimental.pallas import tpu as pltpu
from jax.sharding import PartitionSpec as P

SPAN = 64
EPSILON = 1e-06
NEGATIVE = -1e30
F32 = jnp.float32
BF16 = jnp.bfloat16
MESH = pl.DeviceIdType.MESH
VMEM = pl.BlockSpec(memory_space=pltpu.VMEM)
SMEM = pl.BlockSpec(memory_space=pltpu.SMEM)
ANY = pl.BlockSpec(memory_space=pl.ANY)


def params(cid):
    return pltpu.CompilerParams(
        collective_id=cid, has_side_effects=True, vmem_limit_bytes=56 * 1024 * 1024
    )


def row_norm(value_rows, gain):
    mean_square = jnp.mean(value_rows * value_rows, axis=-1, keepdims=True)
    return value_rows * lax.rsqrt(mean_square + EPSILON) * gain


def meet(axis, n):
    me = lax.axis_index(axis)
    barrier = pltpu.get_barrier_semaphore()
    for k in range(1, n):
        pl.semaphore_signal(
            barrier, inc=1, device_id={axis: lax.rem(me + k, n)}, device_id_type=MESH
        )
    pl.semaphore_wait(barrier, n - 1)


def remote(src, dst, send, recv, axis, peer):
    return pltpu.make_async_remote_copy(
        src_ref=src,
        dst_ref=dst,
        send_sem=send,
        recv_sem=recv,
        device_id={axis: peer},
        device_id_type=MESH,
    )


def dot(a, b):
    return jnp.dot(a, b, preferred_element_type=F32)


def dot_t(a, b):
    return lax.dot_general(a, b, (((1,), (1,)), ((), ())), preferred_element_type=F32)


def dot_0(a, b):
    return lax.dot_general(a, b, (((0,), (0,)), ((), ())), preferred_element_type=F32)


def project_kernel(widths, heads, fold, *refs):
    nw = len(widths)
    x_ref = refs[0]
    weights = refs[1 : 1 + nw]
    rq, rf, ri, rg, kv, qs = refs[1 + nw : 7 + nw]
    xs, wbuf, proj, wsem, ssem, rsem, lsem = refs[7 + nw :]
    rows = x_ref.shape[0]
    me = lax.axis_index("tp")
    a, c = me // 2, lax.rem(me, 2)
    far, sib = (1 - a) * 2 + c, a * 2 + (1 - c)
    offs = [sum(widths[:i]) for i in range(nw)]
    loads = [
        pltpu.make_async_copy(w, wbuf.at[:, pl.ds(o, n)], wsem.at[i])
        for i, (w, o, n) in enumerate(zip(weights, offs, widths))
    ]
    meet("tp", 4)
    pieces = 2
    part = rows // pieces
    cross = []
    for p in range(pieces):
        cp = remote(
            x_ref.at[pl.ds(p * part, part)],
            xs.at[pl.ds(me * rows + p * part, part)],
            ssem.at[p],
            rsem.at[p],
            "tp",
            far,
        )
        cp.start()
        cross.append(cp)
    side = remote(
        x_ref, xs.at[pl.ds(me * rows, rows)], ssem.at[pieces], rsem.at[pieces], "tp", sib
    )
    side.start()
    own = pltpu.make_async_copy(x_ref, xs.at[pl.ds(me * rows, rows)], lsem)
    own.start()
    for load in loads:
        load.start()
    own.wait()
    side.wait()
    for load in loads:
        load.wait()
    tile = 256
    count = sum(widths) // tile

    def group(g):
        base = pl.multiple_of(g * 2 * rows, 2 * rows)

        def one(t, _):
            cols = pl.ds(pl.multiple_of(t * tile, tile), tile)
            proj[pl.ds(base, 2 * rows), cols] = dot(
                xs[pl.ds(base, 2 * rows), :], wbuf[:, cols]
            ).astype(BF16)
            return 0

        lax.fori_loop(0, count, one, 0)

    forward = []
    for p in range(pieces):
        cross[p].wait_recv()
        where = pl.ds(far * rows + p * part, part)
        cp = remote(
            xs.at[where],
            xs.at[where],
            ssem.at[pieces + 1 + p],
            rsem.at[pieces + 1 + p],
            "tp",
            sib,
        )
        cp.start()
        forward.append(cp)
    group(a)
    for cp in forward:
        cp.wait()
    for cp in cross:
        cp.wait_send()
    group(1 - a)
    rq[...] = proj[:, offs[0] : offs[0] + widths[0]]
    rf[...] = proj[:, offs[1] : offs[1] + widths[1]]
    ri[...] = proj[:, offs[2] : offs[2] + widths[2]]
    rg[...] = proj[:, offs[3] : offs[3] + widths[3]]
    pair = widths[4] // heads
    wide = widths[8] // heads
    for h in range(heads):
        kv[h] = jnp.concatenate(
            [
                proj[:, offs[6] + h * pair : offs[6] + (h + 1) * pair],
                proj[:, offs[7] + h * pair : offs[7] + (h + 1) * pair],
                proj[:, offs[8] + h * wide : offs[8] + (h + 1) * wide],
            ],
            axis=1,
        )
        parts = []
        for j in (4, 5):
            scaled = proj[:, offs[j] + h * pair : offs[j] + (h + 1) * pair].astype(F32) * fold
            high = scaled.astype(BF16)
            parts += [high, (scaled - high.astype(F32)).astype(BF16)]
        qs[h] = jnp.concatenate(parts, axis=1)


def recur_kernel(n, heads, rq, rf, ri, kv, qs, floor, shift, *refs):
    local, qdecay, state, total, kv_all, q_all, st, ssem, rsem, lsem = refs
    me = lax.axis_index("sp")
    share = n // heads
    rows = rq.shape[0]
    mine = rows // share
    keys = floor.shape[1] // heads
    width = ri.shape[1] // heads
    meet("sp", n)
    copies = []
    for k in range(1, n):
        peer = lax.rem(me + k, n)
        head, portion = peer // share, lax.rem(peer, share)
        copies.append(
            remote(kv.at[head], kv_all.at[me], ssem.at[0, k], rsem.at[0, k], "sp", peer)
        )
        copies.append(
            remote(
                qs.at[head, pl.ds(pl.multiple_of(portion * mine, mine), mine)],
                q_all.at[me],
                ssem.at[1, k],
                rsem.at[1, k],
                "sp",
                peer,
            )
        )
    for cp in copies:
        cp.start()
    head, portion = me // share, lax.rem(me, share)
    own_kv = pltpu.make_async_copy(kv.at[head], kv_all.at[me], lsem.at[0])
    own_q = pltpu.make_async_copy(
        qs.at[head, pl.ds(pl.multiple_of(portion * mine, mine), mine)], q_all.at[me], lsem.at[1]
    )
    own_kv.start()
    own_q.start()

    st[...] = jnp.zeros_like(st)
    lower = lax.broadcasted_iota(jnp.int32, (SPAN, SPAN), 0) >= lax.broadcasted_iota(
        jnp.int32, (SPAN, SPAN), 1
    )
    ones = jnp.where(lower, 1.0, 0.0).astype(BF16)

    def chunk(i, run):
        at = pl.ds(pl.multiple_of(i * SPAN, SPAN), SPAN)
        key = floor[...] * jax.nn.sigmoid(-rf[at, :].astype(F32))
        moves = shift[at, :]
        decay = jnp.log1p(-key) + jnp.concatenate(
            [jnp.broadcast_to(moves[:, h : h + 1], (SPAN, keys)) for h in range(heads)], axis=1
        )
        high = decay.astype(BF16)
        rest = decay - high.astype(F32)
        mid = rest.astype(BF16)
        low = (rest - mid.astype(F32)).astype(BF16)
        along = dot(ones, high) + dot(ones, mid) + dot(ones, low)
        last = along[SPAN - 1 : SPAN, :]
        query = rq[at, :].astype(F32)
        scaled = query * jnp.exp(along)
        front = scaled.astype(BF16)
        qdecay[at, :] = (query * jnp.exp(along + run)).astype(BF16)
        back = (key * jnp.exp(-along)).astype(BF16)
        push = (key * jnp.exp(last - along)).astype(BF16)
        keep = jnp.exp(last)
        for h in range(heads):
            lanes = slice(h * keys, (h + 1) * keys)
            value = ri[at, h * width : (h + 1) * width]
            score = jnp.where(lower, dot_t(front[:, lanes], back[:, lanes]), 0.0)
            local[at, h * width : (h + 1) * width] = dot(score.astype(BF16), value) + dot_t(
                front[:, lanes], st[h].astype(BF16)
            )
            st[h] = keep[:, lanes] * st[h] + dot_0(value, push[:, lanes])
        return run + last

    run = lax.fori_loop(0, rows // SPAN, chunk, jnp.zeros((1, heads * keys), F32))
    state[...] = st[...].astype(BF16)
    total[...] = jnp.broadcast_to(run, total.shape)
    own_kv.wait()
    own_q.wait()
    for cp in copies:
        cp.wait()


def attend_kernel(n, heads, q_all, kv_all, state, total, lam, gain, *refs):
    msg, incoming, kd, va, states, totals, ssem, rsem = refs
    me = lax.axis_index("sp")
    share = n // heads
    portion = lax.rem(me, share)
    rows = kv_all.shape[1]
    mine = q_all.shape[1]
    width = gain.shape[1]
    pair = (kv_all.shape[2] - width) // 2
    meet("sp", n)

    def copies(k):
        peer = lax.rem(me + k, n)
        return (
            remote(state, states.at[me], ssem.at[0, k], rsem.at[0, k], "sp", peer),
            remote(total, totals.at[me], ssem.at[1, k], rsem.at[1, k], "sp", peer),
        )

    for k in range(1, n):

        @pl.when(me + k < n)
        def _():
            for cp in copies(k):
                cp.start()

    def prepare(b, _):
        block = kv_all[b]
        one, two = block[:, :pair], block[:, pair : 2 * pair]
        kd[b] = jnp.concatenate([one, one, two, two], axis=1)
        va[b] = jnp.concatenate([block[:, 2 * pair :], jnp.ones((rows, width), BF16)], axis=1)
        return 0

    lax.fori_loop(0, n, prepare, 0)
    visible = (
        portion * mine + lax.broadcasted_iota(jnp.int32, (mine, rows), 0)
    ) >= lax.broadcasted_iota(jnp.int32, (mine, rows), 1)

    def block(b, _):
        queries = [q_all[b, :, 0 : 2 * pair], q_all[b, :, 2 * pair : 4 * pair]]

        def step(u, carry, mask):
            out = []
            for j in range(2):
                top, acc = carry[2 * j], carry[2 * j + 1]
                score = dot_t(queries[j], kd[u, :, 2 * pair * j : 2 * pair * (j + 1)])
                if mask:
                    score = jnp.where(visible, score, NEGATIVE)
                newest = jnp.maximum(top, jnp.max(score, axis=1, keepdims=True))
                weight = jnp.exp2(score - newest).astype(BF16)
                out += [newest, acc * jnp.exp2(top - newest) + dot(weight, va[u])]
            return tuple(out)

        first = (
            jnp.full((mine, 1), NEGATIVE, F32),
            jnp.zeros((mine, 2 * width), F32),
        ) * 2
        carry = step(b, first, True)
        top1, acc1, top2, acc2 = lax.fori_loop(0, b, lambda u, s: step(u, s, False), carry)
        sum1, sum2 = acc1[:, width : width + 1], acc2[:, width : width + 1]
        out = acc1[:, :width] / sum1 - lam[0, 0] * (acc2[:, :width] / sum2)
        parts = [row_norm(out, gain[...]).astype(BF16)]
        for top, total_weight in ((top1, sum1), (top2, sum2)):
            value = (top + jnp.log2(total_weight)) * math.log(2.0)
            for _ in range(3):
                piece = value.astype(BF16)
                parts.append(piece)
                value = value - piece.astype(F32)
        parts.append(jnp.zeros((mine, msg.shape[2] - width - 6), BF16))
        msg[b] = jnp.concatenate(parts, axis=1)
        return 0

    lax.fori_loop(0, n, block, 0)

    for k in range(1, n):

        @pl.when(me + k < n)
        def _():
            for cp in copies(k):
                cp.wait_send()

        @pl.when(me >= k)
        def _():
            for cp in copies(k):
                cp.wait_recv()

    incoming[...] = jnp.zeros_like(incoming)
    keys = state.shape[2]

    def join(b, _):
        grow = jnp.exp(totals[b])
        for h in range(heads):
            incoming[h] = grow[0:1, h * keys : (h + 1) * keys] * incoming[h] + states[b, h].astype(
                F32
            )
        return 0

    lax.fori_loop(0, me, join, 0)


def finish_kernel(n, heads, msg, local, qdecay, incoming, gate, gain, *refs):
    mixed, logsum, back, ssem, rsem, lsem = refs
    me = lax.axis_index("sp")
    share = n // heads
    mine = msg.shape[1]
    width = gain.shape[1]
    keys = qdecay.shape[1] // heads
    meet("sp", n)
    copies = []
    for k in range(1, n):
        peer = lax.rem(me + k, n)
        copies.append(remote(msg.at[peer], back.at[me], ssem.at[k], rsem.at[k], "sp", peer))
    for cp in copies:
        cp.start()
    own = pltpu.make_async_copy(msg.at[me], back.at[me], lsem)
    own.start()
    for h in range(heads):
        lanes = slice(h * width, (h + 1) * width)
        value = local[:, lanes] + dot_t(
            qdecay[:, h * keys : (h + 1) * keys], incoming[h].astype(BF16)
        )
        mixed[:, lanes] = (row_norm(value, gain[...]) * jax.nn.silu(gate[:, lanes].astype(F32))).astype(
            BF16
        )
    own.wait()
    for cp in copies:
        cp.wait()
    for h in range(heads):
        for s in range(share):
            block = back[h * share + s]
            where = slice(s * mine, (s + 1) * mine)
            mixed[where, (heads + h) * width : (heads + h + 1) * width] = block[:, :width]
            turned = jnp.transpose(block.astype(F32))
            for j in range(2):
                at = width + 3 * j
                logsum[j, h : h + 1, where] = (
                    turned[at : at + 1] + turned[at + 1 : at + 2]
                ) + turned[at + 2 : at + 3]


def merge_kernel(n, mixed, recur, diff, gain, out, got, rbuf, dbuf, ssem, rsem, lsem):
    me = lax.axis_index("tp")
    rows = out.shape[0]
    half = mixed.shape[1] // 2
    loads = [
        pltpu.make_async_copy(recur, rbuf, lsem.at[1]),
        pltpu.make_async_copy(diff, dbuf, lsem.at[2]),
    ]
    meet("tp", n)
    copies = []
    for k in range(1, n):
        peer = lax.rem(me + k, n)
        copies.append(
            remote(
                mixed.at[pl.ds(pl.multiple_of(peer * rows, rows), rows)],
                got.at[me],
                ssem.at[k],
                rsem.at[k],
                "tp",
                peer,
            )
        )
    for cp in copies:
        cp.start()
    own = pltpu.make_async_copy(
        mixed.at[pl.ds(pl.multiple_of(me * rows, rows), rows)], got.at[me], lsem.at[0]
    )
    own.start()
    for load in loads:
        load.start()
    for load in loads:
        load.wait()
    own.wait()
    for cp in copies:
        cp.wait()
    left = jnp.concatenate([got[g, :, :half] for g in range(n)], axis=1)
    right = jnp.concatenate([got[g, :, half:] for g in range(n)], axis=1)
    merged = dot(left, rbuf[...]) + dot(right, dbuf[...])
    out[...] = row_norm(merged, gain[...]).astype(BF16)


def body(
    tokens,
    input_gain,
    recur_query,
    recur_forget,
    recur_input,
    recur_gate,
    first_query,
    second_query,
    first_key,
    second_key,
    diff_value,
    forget_floor,
    decay_shift,
    recur_gain,
    diff_gain,
    diff_lambda,
    recur_out,
    diff_out,
    final_gain,
):
    groups = lax.axis_size("tp")
    blocks = lax.axis_size("sp")
    heads, keys = forget_floor.shape
    width = recur_gain.shape[0]
    rows = decay_shift.shape[1]
    piece, model = tokens.shape
    share = blocks // heads
    mine = rows // share
    pair = first_query.shape[1] // heads
    assert groups == 4 and blocks % heads == 0 and rows % SPAN == 0
    message = 2 * pair + width
    weights = (
        recur_query,
        recur_forget,
        recur_input,
        recur_gate,
        first_query,
        second_query,
        first_key,
        second_key,
        diff_value,
    )
    widths = tuple(w.shape[1] for w in weights)
    shape = jax.ShapeDtypeStruct
    dma = pltpu.SemaphoreType.DMA
    normed = row_norm(tokens.astype(F32), input_gain).astype(BF16)
    rq, rf, ri, rg, kv, qs = pl.pallas_call(
        functools.partial(
            project_kernel, widths, heads, pair ** (-0.5) / math.log(2.0)
        ),
        out_shape=(
            shape((rows, widths[0]), BF16),
            shape((rows, widths[1]), BF16),
            shape((rows, widths[2]), BF16),
            shape((rows, widths[3]), BF16),
            shape((heads, rows, message), BF16),
            shape((heads, rows, 4 * pair), BF16),
        ),
        in_specs=[VMEM] + [ANY] * len(weights),
        out_specs=(VMEM,) * 6,
        scratch_shapes=[
            pltpu.VMEM((rows, model), BF16),
            pltpu.VMEM((model, sum(widths)), BF16),
            pltpu.VMEM((rows, sum(widths)), BF16),
            dma((len(weights),)),
            dma((5,)),
            dma((5,)),
            dma,
        ],
        compiler_params=params(0),
        name="project",
    )(normed, *weights)
    recur_out, diff_out, kv = lax.optimization_barrier((recur_out, diff_out, kv))
    full_recur = lax.all_gather(recur_out, "tp", axis=0, tiled=True)
    full_diff = lax.all_gather(diff_out, "tp", axis=0, tiled=True)
    local, qdecay, state, total, kv_all, q_all = pl.pallas_call(
        functools.partial(recur_kernel, blocks, heads),
        out_shape=(
            shape((rows, heads * width), F32),
            shape((rows, heads * keys), BF16),
            shape((heads, width, keys), BF16),
            shape((8, heads * keys), F32),
            shape((blocks, rows, message), BF16),
            shape((blocks, mine, 4 * pair), BF16),
        ),
        in_specs=[VMEM] * 7,
        out_specs=(VMEM,) * 6,
        scratch_shapes=[
            pltpu.VMEM((heads, width, keys), F32),
            dma((2, blocks)),
            dma((2, blocks)),
            dma((2,)),
        ],
        compiler_params=params(1),
        name="recur",
    )(rq, rf, ri, kv, qs, forget_floor.reshape(1, heads * keys), jnp.transpose(decay_shift))
    lam = lax.dynamic_slice_in_dim(diff_lambda, lax.axis_index("sp") // share, 1, 0)
    msg, incoming = pl.pallas_call(
        functools.partial(attend_kernel, blocks, heads),
        out_shape=(
            shape((blocks, mine, 2 * width), BF16),
            shape((heads, width, keys), F32),
        ),
        in_specs=[VMEM] * 4 + [SMEM, VMEM],
        out_specs=(VMEM,) * 2,
        scratch_shapes=[
            pltpu.VMEM((blocks, rows, 4 * pair), BF16),
            pltpu.VMEM((blocks, rows, 2 * width), BF16),
            pltpu.VMEM((blocks, heads, width, keys), BF16),
            pltpu.VMEM((blocks, 8, heads * keys), F32),
            dma((2, blocks)),
            dma((2, blocks)),
        ],
        compiler_params=params(2),
        name="attend",
    )(q_all, kv_all, state, total, lam.reshape(1, 1), diff_gain.reshape(1, width))
    mixed, logsum = pl.pallas_call(
        functools.partial(finish_kernel, blocks, heads),
        out_shape=(
            shape((rows, 2 * heads * width), BF16),
            shape((2, heads, rows), F32),
        ),
        in_specs=[VMEM] * 6,
        out_specs=(VMEM,) * 2,
        scratch_shapes=[
            pltpu.VMEM((blocks, mine, 2 * width), BF16),
            dma((blocks,)),
            dma((blocks,)),
            dma,
        ],
        compiler_params=params(3),
        name="finish",
    )(msg, local, qdecay, incoming, rg, recur_gain.reshape(1, width))
    layer_out = pl.pallas_call(
        functools.partial(merge_kernel, groups),
        out_shape=shape((piece, model), BF16),
        in_specs=[VMEM, ANY, ANY, VMEM],
        out_specs=VMEM,
        scratch_shapes=[
            pltpu.VMEM((groups, piece, 2 * heads * width), BF16),
            pltpu.VMEM(full_recur.shape, BF16),
            pltpu.VMEM(full_diff.shape, BF16),
            dma((groups,)),
            dma((groups,)),
            dma((3,)),
        ],
        compiler_params=params(4),
        name="merge",
    )(mixed, full_recur, full_diff, final_gain.reshape(1, model))
    return layer_out, logsum


def solution(mesh):
    in_specs = (
        P(("sp", "tp"), None),
        P(),
        P(None, "tp"),
        P(None, "tp"),
        P(None, "tp"),
        P(None, "tp"),
        P(None, "tp"),
        P(None, "tp"),
        P(None, "tp"),
        P(None, "tp"),
        P(None, "tp"),
        P("tp", None),
        P("tp", "sp"),
        P(),
        P(),
        P("tp"),
        P("tp", None),
        P("tp", None),
        P(),
    )
    out_specs = (P(("sp", "tp"), None), P(None, "tp", "sp"))
    return jax.shard_map(body, mesh=mesh, in_specs=in_specs, out_specs=out_specs, check_vma=False)
```

time: 416 us -> 159 us (0.38)
  matrix products: 198 us -> 0 us
  Pallas kernels: 0 us -> 136 us
  local copies, waits for them, and re-layouts: 73.7 us -> 3.94 us
  other arithmetic: 60.2 us -> 3.27 us
  blocking collectives: 40.2 us -> 0 us
  starting transfers between devices: 14.5 us -> 0.08 us
  waiting for transfers between devices: 10.9 us -> 0.75 us
    dot_general x51 -> x0, matrix products: 198 us -> none  [the longest x8 125 us: block_step(): jnp.einsum('htk,htsk,hsk->hts', query_vector, factors, keyed_values, prec...]
    pallas_call x0 -> x5, Pallas kernels: none -> 136 us  [the longest x1 40.3 us: body(): pl.pallas_call(functools.partial(recur_kernel, blocks, heads), out_shape=...]
    all_gather x2 -> x0, blocking collectives: 40.2 us -> none  [entering(): lax.all_gather(a.astype(kind), axis)]
    convert_element_type x11 -> x1, other arithmetic: 31.9 us -> 2.03 us  [body(): normed = row_norm(tokens.astype(F32), input_gain).astype(BF16)]
    slice x29 -> x0, local copies, waits for them, and re-layouts: 17 us -> none  [the longest x8 7.94 us: update(): block[:, :small].reshape(step, heads, pair_width)]
    unnamed x39 -> x9, local copies, waits for them, and re-layouts: 20.1 us -> 3.36 us
    all_to_all x1 -> x0, starting transfers between devices: 14.4 us -> none  [body(): moved = lax.all_to_all(mixed, 'tp', split_axis=0, concat_axis=1, tiled=True)]
    dynamic_slice x22 -> x1, local copies, waits for them, and re-layouts: 14.2 us -> 0.58 us  [body(): lax.dynamic_slice_in_dim(diff_lambda, lax.axis_index('sp') // share, 1, 0)]
  transfers between devices with their start and end apart: 5 -> 2, of which waited for: 1 -> 0; matrix products, arithmetic and copies ran while one was open for 75% -> 1% of each run, Pallas kernels for 0% -> 60%
where the time goes in v1:
time: 159 us; the launch traced here: 158 us
  Pallas kernels  136 us (86%)
  between operations  14.1 us (9%)
  local copies, waits for them, and re-layouts  3.94 us (2%)
  other arithmetic  3.27 us (2%)
    pallas_call x1, Pallas kernels, body(): pl.pallas_call(functools.partial(recur_kernel, blocks, heads), out_shape=...  40.3 us
    pallas_call x1, Pallas kernels, body(): pl.pallas_call(functools.partial(attend_kernel, blocks, heads), out_shape...  39.3 us
    pallas_call x1, Pallas kernels, body(): pl.pallas_call(functools.partial(project_kernel, widths, heads, pair ** (...  25.8 us
    pallas_call x1, Pallas kernels, body(): pl.pallas_call(functools.partial(finish_kernel, blocks, heads), out_shape...  15.2 us
    pallas_call x1, Pallas kernels, body(): pl.pallas_call(functools.partial(merge_kernel, groups), out_shape=shape((...  15.1 us
    unnamed x9, local copies, waits for them, and re-layouts  3.36 us
  transfers between devices with their start and end apart: 2, of which 0 were waited for; matrix products, arithmetic and copies ran while one was open for 1% of the time, Pallas kernels for 60%

profile of v1, /device:TPU:31, one launch (start us, length us, event | category | flops | bytes accessed | tf_op | source)
XLA Modules:
  0.0 157.8 jit_solution(5652996936265606845)
XLA Ops:
  7.2 0.0 all-gather.3.cloned.1.call-start
  7.2 1.2 fusion
  8.4 2.0 %fusion.2.refs_0_ = bf16[128,2048]{1,0:T(8,128)(2,1)} fusion(bf16[128,2048]{1,0:T(8,128)(2,1)} %param.19, f32[2048]{0:T(1024)} %param.20, f32[128]{0:T(128)S(1)} %add_rsqrt_fusion), kind=kLoop, calls=%fused_computation.4 | loop fusion | flops 1048576 | bytes 1057280 | tf_op jit(solution)/shard_map/convert_element_type | solution.py:473
  10.5 0.0 copy-start.1
  10.5 0.0 copy-start.2
  10.5 25.8 %project.1 = (bf16[512,512]{1,0:T(8,128)(2,1)}, bf16[512,512]{1,0:T(8,128)(2,1)}, bf16[512,256]{1,0:T(8,128)(2,1)}, bf16[512,256]{1,0:T(8,128)(2,1)}, bf16[4,512...) custom-call(bf16[128,2048]{1,0:T(8,128)(2,1)} %fusion.2.refs_0_, bf16[2048,512]{1,0:T(8,128)(2,1)} %refs_1_.1, ...), custom_call_target="tpu_custom_call" | custom-call | tf_op jit(solution)/shard_map/project/pallas_call | solution.py:474
  36.3 0.0 all-gather.3.cloned.1.call-update
  36.3 0.0 all-gather.5.cloned.1.call-start
  36.4 0.7 all-gather.5.cloned.1.call-update
  37.1 0.0 copy-done.1
  37.1 0.9 copy.21
  38.0 0.0 copy-done.2
  38.0 0.6 dynamic_slice.3
  38.6 40.3 %recur.1 = (f32[512,256]{1,0:T(8,128)}, bf16[512,512]{1,0:T(8,128)(2,1)}, bf16[4,64,128]{2,1,0:T(8,128)(2,1)}, f32[8,512]{1,0:T(8,128)}, bf16[8,512,128]{2,1,0:T(8,128)(2,1)}, /*index=5*/bf16[8,256,128]{2,1,0:T(8,128)(2,1)}) custom-call(bf16[512,512]{1,0:T(8,128)(2,1)} %get-tuple-element.21.rq, bf16[512,512]{1,0:T(8,128)(2,1)} %get-tuple-element.22.rf, ...), custom_call_target="tpu_custom_call" | custom-call | tf_op jit(solution)/shard_map/recur/pallas_call | solution.py:503
  78.8 39.3 %attend.1 = (bf16[8,256,128]{2,1,0:T(8,128)(2,1)}, f32[4,64,128]{2,1,0:T(8,128)}) custom-call(bf16[8,256,128]{2,1,0:T(8,128)(2,1)} %get-tuple-element.27.q_all, bf16[8,512,128]{2,1,0:T(8,128)(2,1)} %get-tuple-element.28.kv_all, bf16[4,64,128]{2,1,0:T(8,128)(2,1)} %get-tuple-element.29.state, f32[8,512]{1,0:T(8,128)} %get-tuple-element.30.total, ...), custom_call_target="tpu_custom_call" | custom-call | tf_op jit(solution)/shard_map/attend/pallas_call | solution.py:525
  118.1 15.2 %finish.1 = (bf16[512,512]{1,0:T(8,128)(2,1)}, f32[2,4,512]{2,1,0:T(4,128)}) custom-call(bf16[8,256,128]{2,1,0:T(8,128)(2,1)} %get-tuple-element.31.msg, f32[512,256]{1,0:T(8,128)} %get-tuple-element.32.local, bf16[512,512]{1,0:T(8,128)(2,1)} %get-tuple-element.33.qdecay, f32[4,64,128]{2,1,0:T(8,128)} %get-tuple-element.34.incoming, ...), custom_call_target="tpu_custom_call" | custom-call | tf_op jit(solution)/shard_map/finish/pallas_call | solution.py:544
  133.3 0.0 all-gather.3.cloned.1.call-done.recur
  133.4 0.0 all-gather.5.cloned.1.call-done.diff
  133.4 0.0 copy-start
  133.4 15.1 %merge.1 = bf16[128,2048]{1,0:T(8,128)(2,1)} custom-call(bf16[512,512]{1,0:T(8,128)(2,1)} %get-tuple-element.36.mixed, bf16[1024,2048]{1,0:T(8,128)(2,1)} %all-gather.3.cloned.1.call-done.recur, bf16[1024,2048]{1,0:T(8,128)(2,1)} %all-gather.5.cloned.1.call-done.diff, f32[1,2048]{1,0:T(1,128)} %bitcast.7), custom_call_target="tpu_custom_call" | custom-call | tf_op jit(solution)/shard_map/merge/pallas_call | solution.py:561
  148.5 1.9 %copy.24 = bf16[128,2048]{1,0:T(8,128)(2,1)} copy(bf16[128,2048]{1,0:T(8,128)(2,1)} %merge.1) | data formatting | bytes 1048576
  150.4 0.0 copy-done
  150.4 0.6 copy.25
  (1 shorter events, 0.0 us)
Async XLA Ops:
  7.2 126.2 %all-gather.3.cloned.1.call-start = ((), (), s32[]{:S(2)}) async-start(), calls=%async_computation | async-start | bytes 5242880 | tf_op jit(solution)/shard_map/all_gather | solution.py:501
  10.5 26.6 %copy-start.1 = (f32[4,512]{1,0:T(4,128)S(1)}, f32[4,512]{1,0:T(4,128)}, u32[]{:S(2)}) copy-start(f32[4,512]{1,0:T(4,128)} %param.31) | copy-start | bytes 24580
  10.5 27.5 %copy-start.2 = (f32[4]{0:T(128)S(1)}, f32[4]{0:T(128)}, u32[]{:S(2)}) copy-start(f32[4]{0:T(128)} %param.34) | copy-start | bytes 52
  36.3 97.0 %all-gather.5.cloned.1.call-start = ((), (), s32[]{:S(2)}) async-start(), calls=%async_computation.1 | async-start | bytes 5242880 | tf_op jit(solution)/shard_map/all_gather | solution.py:502
  133.4 17.0 %copy-start = (f32[2,4,512]{2,1,0:T(4,128)S(1)}, f32[2,4,512]{2,1,0:T(4,128)}, u32[]{:S(2)}) copy-start(f32[2,4,512]{2,1,0:T(4,128)} %get-tuple-element.43) | copy-start | bytes 49156
Sparse Core Ops, SparseCore 0:
  36.5 35.1 all-gather.2
  73.2 34.4 all-gather.4

commit v2 on v1

v2 whole, which is shorter than its diff:
```python
import functools
import math

import jax
import jax.numpy as jnp
from jax import lax
from jax.experimental import pallas as pl
from jax.experimental.pallas import tpu as pltpu
from jax.sharding import PartitionSpec as P

SPAN = 64
EPSILON = 1e-06
NEGATIVE = -1e30
F32 = jnp.float32
BF16 = jnp.bfloat16
MESH = pl.DeviceIdType.MESH
VMEM = pl.BlockSpec(memory_space=pltpu.VMEM)
SMEM = pl.BlockSpec(memory_space=pltpu.SMEM)
ANY = pl.BlockSpec(memory_space=pl.ANY)


def params(cid):
    return pltpu.CompilerParams(
        collective_id=cid, has_side_effects=True, vmem_limit_bytes=56 * 1024 * 1024
    )


def row_norm(value_rows, gain):
    mean_square = jnp.mean(value_rows * value_rows, axis=-1, keepdims=True)
    return value_rows * lax.rsqrt(mean_square + EPSILON) * gain


def around():
    me = lax.axis_index("tp")
    a, c = me // 2, lax.rem(me, 2)
    return me, (1 - a) * 2 + c, a * 2 + (1 - c), (1 - a) * 2 + (1 - c)


def meet(axis, n, *others):
    me = lax.axis_index(axis)
    barrier = pltpu.get_barrier_semaphore()
    for k in range(1, n):
        pl.semaphore_signal(
            barrier, inc=1, device_id={axis: lax.rem(me + k, n)}, device_id_type=MESH
        )
    for other in others:
        pl.semaphore_signal(barrier, inc=1, device_id={"tp": other}, device_id_type=MESH)
    pl.semaphore_wait(barrier, n - 1 + len(others))


def remote(src, dst, send, recv, axis, peer):
    return pltpu.make_async_remote_copy(
        src_ref=src,
        dst_ref=dst,
        send_sem=send,
        recv_sem=recv,
        device_id={axis: peer},
        device_id_type=MESH,
    )


def dot(a, b):
    return jnp.dot(a, b, preferred_element_type=F32)


def dot_t(a, b):
    return lax.dot_general(a, b, (((1,), (1,)), ((), ())), preferred_element_type=F32)


def dot_0(a, b):
    return lax.dot_general(a, b, (((0,), (0,)), ((), ())), preferred_element_type=F32)


def project_kernel(widths, heads, *refs):
    nw = len(widths)
    x_ref, gain = refs[:2]
    weights = refs[2 : 2 + nw]
    rq, rf, ri, rg, kv, qs = refs[2 + nw : 8 + nw]
    xs, xn, wbuf, proj, wsem, ssem, rsem, lsem = refs[8 + nw :]
    rows = x_ref.shape[0]
    me, far, sib, _ = around()
    a = me // 2
    offs = [sum(widths[:i]) for i in range(nw)]
    loads = [
        pltpu.make_async_copy(w, wbuf.at[:, pl.ds(o, n)], wsem.at[i])
        for i, (w, o, n) in enumerate(zip(weights, offs, widths))
    ]
    own = pltpu.make_async_copy(x_ref, xs.at[pl.ds(me * rows, rows)], lsem)
    own.start()
    meet("tp", 4)
    pieces = 4
    part = rows // pieces
    cross = []
    for p in range(pieces):
        cp = remote(
            x_ref.at[pl.ds(p * part, part)],
            xs.at[pl.ds(me * rows + p * part, part)],
            ssem.at[p],
            rsem.at[p],
            "tp",
            far,
        )
        cp.start()
        cross.append(cp)
    side = remote(
        x_ref, xs.at[pl.ds(me * rows, rows)], ssem.at[pieces], rsem.at[pieces], "tp", sib
    )
    side.start()
    for load in loads:
        load.start()
    tile = 256
    count = sum(widths) // tile
    band = 2 * rows
    pair = widths[4] // heads
    wide = widths[8] // heads
    mine = 2 * qs.shape[2]
    half = mine // 2

    def normalize(g):
        def one(i, _):
            at = pl.multiple_of(g * band + i * 32, 32)
            value = xs[pl.ds(at, 32), :].astype(F32)
            xn[pl.ds(pl.multiple_of(i * 32, 32), 32), :] = row_norm(value, gain[...]).astype(BF16)
            return 0

        lax.fori_loop(0, band // 32, one, 0)

    def group(g):
        base = pl.multiple_of(g * band, band)

        def one(t, _):
            cols = pl.ds(pl.multiple_of(t * tile, tile), tile)
            proj[:, cols] = dot(xn[...], wbuf[:, cols]).astype(BF16)
            return 0

        lax.fori_loop(0, count, one, 0)
        at = pl.ds(base, band)
        for ref, k in ((rq, 0), (rf, 1), (ri, 2), (rg, 3)):
            ref[at, :] = proj[:, offs[k] : offs[k] + widths[k]]
        for h in range(heads):
            kv[h, at, :] = jnp.concatenate(
                [
                    proj[:, offs[6] + h * pair : offs[6] + (h + 1) * pair],
                    proj[:, offs[7] + h * pair : offs[7] + (h + 1) * pair],
                    proj[:, offs[8] + h * wide : offs[8] + (h + 1) * wide],
                ],
                axis=1,
            )
            for i in range(band // mine):
                parts = []
                for start in (i * mine, i * mine + half):
                    for k in (4, 5):
                        parts.append(
                            proj[
                                start : start + half,
                                offs[k] + h * pair : offs[k] + (h + 1) * pair,
                            ]
                        )
                qs[h, g * (band // mine) + i] = jnp.concatenate(parts, axis=1)

    own.wait()
    side.wait()
    normalize(a)
    for load in loads:
        load.wait()
    group(a)
    forward = []
    for p in range(pieces):
        cross[p].wait_recv()
        where = pl.ds(far * rows + p * part, part)
        cp = remote(
            xs.at[where],
            xs.at[where],
            ssem.at[pieces + 1 + p],
            rsem.at[pieces + 1 + p],
            "tp",
            sib,
        )
        cp.start()
        forward.append(cp)
    for cp in forward:
        cp.wait()
    for cp in cross:
        cp.wait_send()
    normalize(1 - a)
    group(1 - a)


def recur_kernel(n, heads, rq, rf, ri, kv, qs, floor, shift, own_r, *refs):
    local, qdecay, state, total, kv_all, q_all, far_r, st, ssem, rsem, lsem, xsem = refs
    _, far, _, _ = around()
    me = lax.axis_index("sp")
    share = n // heads
    rows = rq.shape[0]
    keys = floor.shape[1] // heads
    width = ri.shape[1] // heads
    meet("sp", n, far)
    copies = []
    for k in range(1, n):
        peer = lax.rem(me + k, n)
        head, portion = peer // share, lax.rem(peer, share)
        copies.append(
            remote(kv.at[head], kv_all.at[me], ssem.at[0, k], rsem.at[0, k], "sp", peer)
        )
        copies.append(
            remote(
                qs.at[head, portion],
                q_all.at[me],
                ssem.at[1, k],
                rsem.at[1, k],
                "sp",
                peer,
            )
        )
    copies.append(remote(own_r, far_r, xsem.at[0], xsem.at[1], "tp", far))
    for cp in copies:
        cp.start()
    head, portion = me // share, lax.rem(me, share)
    own_kv = pltpu.make_async_copy(kv.at[head], kv_all.at[me], lsem.at[0])
    own_q = pltpu.make_async_copy(qs.at[head, portion], q_all.at[me], lsem.at[1])
    own_kv.start()
    own_q.start()

    st[...] = jnp.zeros_like(st)
    lower = lax.broadcasted_iota(jnp.int32, (SPAN, SPAN), 0) >= lax.broadcasted_iota(
        jnp.int32, (SPAN, SPAN), 1
    )
    ones = jnp.where(lower, 1.0, 0.0).astype(BF16)

    def chunk(i, run):
        at = pl.ds(pl.multiple_of(i * SPAN, SPAN), SPAN)
        key = floor[...] * jax.nn.sigmoid(-rf[at, :].astype(F32))
        moves = shift[at, :]
        decay = jnp.log1p(-key) + jnp.concatenate(
            [jnp.broadcast_to(moves[:, h : h + 1], (SPAN, keys)) for h in range(heads)], axis=1
        )
        high = decay.astype(BF16)
        rest = decay - high.astype(F32)
        mid = rest.astype(BF16)
        low = (rest - mid.astype(F32)).astype(BF16)
        along = dot(ones, high) + dot(ones, mid) + dot(ones, low)
        last = along[SPAN - 1 : SPAN, :]
        query = rq[at, :].astype(F32)
        scaled = query * jnp.exp(along)
        front = scaled.astype(BF16)
        qdecay[at, :] = (query * jnp.exp(along + run)).astype(BF16)
        back = (key * jnp.exp(-along)).astype(BF16)
        push = (key * jnp.exp(last - along)).astype(BF16)
        keep = jnp.exp(last)
        for h in range(heads):
            lanes = slice(h * keys, (h + 1) * keys)
            value = ri[at, h * width : (h + 1) * width]
            score = jnp.where(lower, dot_t(front[:, lanes], back[:, lanes]), 0.0)
            local[at, h * width : (h + 1) * width] = dot(score.astype(BF16), value) + dot_t(
                front[:, lanes], st[h].astype(BF16)
            )
            st[h] = keep[:, lanes] * st[h] + dot_0(value, push[:, lanes])
        return run + last

    run = lax.fori_loop(0, rows // SPAN, chunk, jnp.zeros((1, heads * keys), F32))
    state[...] = st[...].astype(BF16)
    total[...] = jnp.broadcast_to(run, total.shape)
    own_kv.wait()
    own_q.wait()
    for cp in copies:
        cp.wait()


def attend_kernel(n, heads, fold, q_all, kv_all, state, total, lam, gain, own_r, far_r, own_d, *refs):
    msg, lmsg, incoming, sib_r, diag_r, far_d, sib_d = refs[:7]
    kt, va, sc, states, totals, ssem, rsem, xsem, ysem = refs[7:]
    me = lax.axis_index("sp")
    _, far, sib, _ = around()
    share = n // heads
    portion = lax.rem(me, share)
    rows = kv_all.shape[1]
    mine = 2 * q_all.shape[1]
    width = gain.shape[1]
    pair = (kv_all.shape[2] - width) // 2
    meet("sp", n, far, sib)

    def copies(k):
        peer = lax.rem(me + k, n)
        return (
            remote(state, states.at[me], ssem.at[0, k], rsem.at[0, k], "sp", peer),
            remote(total, totals.at[me], ssem.at[1, k], rsem.at[1, k], "sp", peer),
        )

    for k in range(1, n):

        @pl.when(me + k < n)
        def _():
            for cp in copies(k):
                cp.start()

    moves = [
        remote(own_d, far_d, xsem.at[0], ysem.at[0], "tp", far),
        remote(own_r, sib_r, xsem.at[1], ysem.at[1], "tp", sib),
        remote(far_r, diag_r, xsem.at[2], ysem.at[2], "tp", sib),
        remote(own_d, sib_d, xsem.at[3], ysem.at[3], "tp", sib),
    ]
    for cp in moves:
        cp.start()

    def prepare(b, _):
        block = kv_all[b]
        turned = jnp.transpose(block.astype(F32)).astype(BF16)
        one, two = turned[:pair], turned[pair : 2 * pair]
        kt[b] = jnp.concatenate([one, one, two, two], axis=0)
        va[b] = jnp.concatenate([block[:, 2 * pair :], jnp.ones((rows, width), BF16)], axis=1)
        return 0

    lax.fori_loop(0, n, prepare, 0)
    lanes = 128

    def block(b, _):
        packed = q_all[b]
        both = jnp.concatenate([packed[:, : 2 * pair], packed[:, 2 * pair :]], axis=0)
        scaled = both.astype(F32) * fold
        high = scaled.astype(BF16)
        low = (scaled - high.astype(F32)).astype(BF16)
        queries = [
            jnp.concatenate(
                [high[:, j * pair : (j + 1) * pair], low[:, j * pair : (j + 1) * pair]], axis=1
            )
            for j in range(2)
        ]

        def score(u, tops, mask):
            out = []
            for j in range(2):
                value = dot(queries[j], kt[u, 2 * pair * j : 2 * pair * (j + 1), :])
                if mask:
                    visible = (
                        portion * mine + lax.broadcasted_iota(jnp.int32, (mine, rows), 0)
                    ) >= lax.broadcasted_iota(jnp.int32, (mine, rows), 1)
                    value = jnp.where(visible, value, NEGATIVE)
                sc[j, u] = value
                top = tops[j]
                for i in range(rows // lanes):
                    top = jnp.maximum(top, value[:, i * lanes : (i + 1) * lanes])
                out.append(top)
            return tuple(out)

        tops = score(b, (jnp.full((mine, lanes), NEGATIVE, F32),) * 2, True)
        tops = lax.fori_loop(0, b, lambda u, t: score(u, t, False), tops)
        tops = [jnp.max(top, axis=1, keepdims=True) for top in tops]
        wide = [jnp.broadcast_to(top, (mine, lanes)) for top in tops]

        def weigh(u, accs):
            out = []
            for j in range(2):
                weight = jnp.concatenate(
                    [
                        jnp.exp2(sc[j, u, :, i * lanes : (i + 1) * lanes] - wide[j]).astype(BF16)
                        for i in range(rows // lanes)
                    ],
                    axis=1,
                )
                out.append(accs[j] + dot(weight, va[u]))
            return tuple(out)

        acc1, acc2 = lax.fori_loop(0, b + 1, weigh, (jnp.zeros((mine, 2 * width), F32),) * 2)
        sum1, sum2 = acc1[:, width : width + 1], acc2[:, width : width + 1]
        out = acc1[:, :width] / sum1 - lam[0, 0] * (acc2[:, :width] / sum2)
        out = row_norm(out, gain[...]).astype(BF16)
        msg[b] = jnp.concatenate([out[: mine // 2], out[mine // 2 :]], axis=1)
        log1 = (tops[0] + jnp.log2(sum1)) * math.log(2.0)
        log2 = (tops[1] + jnp.log2(sum2)) * math.log(2.0)
        lane = lax.broadcasted_iota(jnp.int32, (mine, lanes), 1)
        lmsg[b] = jnp.transpose(jnp.where(lane == 0, log1, log2))[:8]
        return 0

    lax.fori_loop(0, n, block, 0)

    for k in range(1, n):

        @pl.when(me + k < n)
        def _():
            for cp in copies(k):
                cp.wait_send()

        @pl.when(me >= k)
        def _():
            for cp in copies(k):
                cp.wait_recv()

    incoming[...] = jnp.zeros_like(incoming)
    keys = state.shape[2]

    def join(b, _):
        grow = jnp.exp(totals[b])
        for h in range(heads):
            incoming[h] = grow[0:1, h * keys : (h + 1) * keys] * incoming[h] + states[b, h].astype(
                F32
            )
        return 0

    lax.fori_loop(0, me, join, 0)
    for cp in moves:
        cp.wait()


def finish_kernel(n, heads, msg, lmsg, local, qdecay, incoming, gate, gain, far_d, *refs):
    mixed, logsum, diag_d, back, lback, ssem, rsem, lsem, xsem = refs
    me = lax.axis_index("sp")
    _, _, sib, _ = around()
    share = n // heads
    half = msg.shape[1]
    mine = 2 * half
    width = gain.shape[1]
    keys = qdecay.shape[1] // heads
    meet("sp", n, sib)
    copies = []
    for k in range(1, n):
        peer = lax.rem(me + k, n)
        copies.append(
            remote(msg.at[peer], back.at[me], ssem.at[0, k], rsem.at[0, k], "sp", peer)
        )
        copies.append(
            remote(lmsg.at[peer], lback.at[me], ssem.at[1, k], rsem.at[1, k], "sp", peer)
        )
    copies.append(remote(far_d, diag_d, xsem.at[0], xsem.at[1], "tp", sib))
    for cp in copies:
        cp.start()
    own = pltpu.make_async_copy(msg.at[me], back.at[me], lsem.at[0])
    own_l = pltpu.make_async_copy(lmsg.at[me], lback.at[me], lsem.at[1])
    own.start()
    own_l.start()
    for h in range(heads):
        lanes = slice(h * width, (h + 1) * width)
        value = local[:, lanes] + dot_t(
            qdecay[:, h * keys : (h + 1) * keys], incoming[h].astype(BF16)
        )
        mixed[:, lanes] = (row_norm(value, gain[...]) * jax.nn.silu(gate[:, lanes].astype(F32))).astype(
            BF16
        )
    own.wait()
    own_l.wait()
    for cp in copies:
        cp.wait()
    for h in range(heads):
        lanes = slice((heads + h) * width, (heads + h + 1) * width)
        for s in range(share):
            block = back[h * share + s]
            mixed[s * mine : s * mine + half, lanes] = block[:, :width]
            mixed[s * mine + half : (s + 1) * mine, lanes] = block[:, width:]
            for j in range(2):
                logsum[j, h : h + 1, s * mine : (s + 1) * mine] = lback[h * share + s, j : j + 1, :]


def merge_kernel(n, mixed, gain, *refs):
    sources = refs[:8]
    out, got, rbuf, dbuf, ssem, rsem, lsem, wsem = refs[8:]
    me, *rest = around()
    rows = out.shape[0]
    half = mixed.shape[1] // 2
    loads = []
    for i, source in enumerate(sources):
        place = (me, *rest)[i % 4]
        into = (rbuf, dbuf)[i // 4]
        loads.append(
            pltpu.make_async_copy(
                source, into.at[pl.ds(pl.multiple_of(place * half, half), half)], wsem.at[i]
            )
        )
    for load in loads:
        load.start()
    meet("tp", n)
    copies = []
    for k in range(1, n):
        peer = lax.rem(me + k, n)
        copies.append(
            remote(
                mixed.at[pl.ds(pl.multiple_of(peer * rows, rows), rows)],
                got.at[me],
                ssem.at[k],
                rsem.at[k],
                "tp",
                peer,
            )
        )
    for cp in copies:
        cp.start()
    own = pltpu.make_async_copy(
        mixed.at[pl.ds(pl.multiple_of(me * rows, rows), rows)], got.at[me], lsem
    )
    own.start()
    for load in loads:
        load.wait()
    own.wait()
    for cp in copies:
        cp.wait()
    left = jnp.concatenate([got[g, :, :half] for g in range(n)], axis=1)
    right = jnp.concatenate([got[g, :, half:] for g in range(n)], axis=1)
    merged = dot(left, rbuf[...]) + dot(right, dbuf[...])
    out[...] = row_norm(merged, gain[...]).astype(BF16)


def body(
    tokens,
    input_gain,
    recur_query,
    recur_forget,
    recur_input,
    recur_gate,
    first_query,
    second_query,
    first_key,
    second_key,
    diff_value,
    forget_floor,
    decay_shift,
    recur_gain,
    diff_gain,
    diff_lambda,
    recur_out,
    diff_out,
    final_gain,
):
    groups = lax.axis_size("tp")
    blocks = lax.axis_size("sp")
    heads, keys = forget_floor.shape
    width = recur_gain.shape[0]
    rows = decay_shift.shape[1]
    piece, model = tokens.shape
    share = blocks // heads
    mine = rows // share
    pair = first_query.shape[1] // heads
    assert groups == 4 and blocks % heads == 0 and rows % SPAN == 0
    message = 2 * pair + width
    weights = (
        recur_query,
        recur_forget,
        recur_input,
        recur_gate,
        first_query,
        second_query,
        first_key,
        second_key,
        diff_value,
    )
    widths = tuple(w.shape[1] for w in weights)
    shape = jax.ShapeDtypeStruct
    dma = pltpu.SemaphoreType.DMA
    rq, rf, ri, rg, kv, qs = pl.pallas_call(
        functools.partial(project_kernel, widths, heads),
        out_shape=(
            shape((rows, widths[0]), BF16),
            shape((rows, widths[1]), BF16),
            shape((rows, widths[2]), BF16),
            shape((rows, widths[3]), BF16),
            shape((heads, rows, message), BF16),
            shape((heads, share, mine // 2, 4 * pair), BF16),
        ),
        in_specs=[ANY, VMEM] + [ANY] * len(weights),
        out_specs=(VMEM,) * 6,
        scratch_shapes=[
            pltpu.VMEM((rows, model), BF16),
            pltpu.VMEM((2 * piece, model), BF16),
            pltpu.VMEM((model, sum(widths)), BF16),
            pltpu.VMEM((2 * piece, sum(widths)), BF16),
            dma((len(weights),)),
            dma((9,)),
            dma((9,)),
            dma,
        ],
        compiler_params=params(0),
        name="project",
    )(tokens, input_gain.reshape(1, model), *weights)
    local, qdecay, state, total, kv_all, q_all, far_r = pl.pallas_call(
        functools.partial(recur_kernel, blocks, heads),
        out_shape=(
            shape((rows, heads * width), F32),
            shape((rows, heads * keys), BF16),
            shape((heads, width, keys), BF16),
            shape((8, heads * keys), F32),
            shape((blocks, rows, message), BF16),
            shape((blocks, mine // 2, 4 * pair), BF16),
            shape(recur_out.shape, BF16),
        ),
        in_specs=[VMEM] * 7 + [ANY],
        out_specs=(VMEM,) * 6 + (ANY,),
        scratch_shapes=[
            pltpu.VMEM((heads, width, keys), F32),
            dma((2, blocks)),
            dma((2, blocks)),
            dma((2,)),
            dma((2,)),
        ],
        compiler_params=params(1),
        name="recur",
    )(
        rq,
        rf,
        ri,
        kv,
        qs,
        forget_floor.reshape(1, heads * keys),
        jnp.transpose(decay_shift),
        recur_out,
    )
    lam = lax.dynamic_slice_in_dim(diff_lambda, lax.axis_index("sp") // share, 1, 0)
    msg, lmsg, incoming, sib_r, diag_r, far_d, sib_d = pl.pallas_call(
        functools.partial(attend_kernel, blocks, heads, pair ** (-0.5) / math.log(2.0)),
        out_shape=(
            shape((blocks, mine // 2, 2 * width), BF16),
            shape((blocks, 8, mine), F32),
            shape((heads, width, keys), F32),
        )
        + (shape(recur_out.shape, BF16),) * 4,
        in_specs=[VMEM] * 4 + [SMEM, VMEM] + [ANY] * 3,
        out_specs=(VMEM,) * 3 + (ANY,) * 4,
        scratch_shapes=[
            pltpu.VMEM((blocks, 4 * pair, rows), BF16),
            pltpu.VMEM((blocks, rows, 2 * width), BF16),
            pltpu.VMEM((2, blocks, mine, rows), F32),
            pltpu.VMEM((blocks, heads, width, keys), BF16),
            pltpu.VMEM((blocks, 8, heads * keys), F32),
            dma((2, blocks)),
            dma((2, blocks)),
            dma((4,)),
            dma((4,)),
        ],
        compiler_params=params(2),
        name="attend",
    )(
        q_all,
        kv_all,
        state,
        total,
        lam.reshape(1, 1),
        diff_gain.reshape(1, width),
        recur_out,
        far_r,
        diff_out,
    )
    mixed, logsum, diag_d = pl.pallas_call(
        functools.partial(finish_kernel, blocks, heads),
        out_shape=(
            shape((rows, 2 * heads * width), BF16),
            shape((2, heads, rows), F32),
            shape(diff_out.shape, BF16),
        ),
        in_specs=[VMEM] * 7 + [ANY],
        out_specs=(VMEM,) * 2 + (ANY,),
        scratch_shapes=[
            pltpu.VMEM((blocks, mine // 2, 2 * width), BF16),
            pltpu.VMEM((blocks, 8, mine), F32),
            dma((2, blocks)),
            dma((2, blocks)),
            dma((2,)),
            dma((2,)),
        ],
        compiler_params=params(3),
        name="finish",
    )(msg, lmsg, local, qdecay, incoming, rg, recur_gain.reshape(1, width), far_d)
    full = shape((groups * heads * width, model), BF16)
    layer_out = pl.pallas_call(
        functools.partial(merge_kernel, groups),
        out_shape=shape((piece, model), BF16),
        in_specs=[VMEM, VMEM] + [ANY] * 8,
        out_specs=VMEM,
        scratch_shapes=[
            pltpu.VMEM((groups, piece, 2 * heads * width), BF16),
            pltpu.VMEM(full.shape, BF16),
            pltpu.VMEM(full.shape, BF16),
            dma((groups,)),
            dma((groups,)),
            dma,
            dma((8,)),
        ],
        compiler_params=params(4),
        name="merge",
    )(
        mixed,
        final_gain.reshape(1, model),
        recur_out,
        far_r,
        sib_r,
        diag_r,
        diff_out,
        far_d,
        sib_d,
        diag_d,
    )
    return layer_out, logsum


def solution(mesh):
    in_specs = (
        P(("sp", "tp"), None),
        P(),
        P(None, "tp"),
        P(None, "tp"),
        P(None, "tp"),
        P(None, "tp"),
        P(None, "tp"),
        P(None, "tp"),
        P(None, "tp"),
        P(None, "tp"),
        P(None, "tp"),
        P("tp", None),
        P("tp", "sp"),
        P(),
        P(),
        P("tp"),
        P("tp", None),
        P("tp", None),
        P(),
    )
    out_specs = (P(("sp", "tp"), None), P(None, "tp", "sp"))
    return jax.shard_map(body, mesh=mesh, in_specs=in_specs, out_specs=out_specs, check_vma=False)
```

time: 159 us -> 127 us (0.80); the launches traced: 158 us -> 124 us
  Pallas kernels: 136 us -> 118 us
  between operations: 14.1 us -> 0.7 us
  other arithmetic: 3.27 us -> 0 us
    pallas_call x2, Pallas kernels: 65.1 us -> 56.6 us  [the longest x1 32.9 us: body(): pl.pallas_call(functools.partial(attend_kernel, blocks, heads, pair ** (-...]
    pallas_call x1, Pallas kernels: 40.3 us -> 35.4 us  [body(): pl.pallas_call(functools.partial(recur_kernel, blocks, heads), out_shape=...]
    pallas_call x1, Pallas kernels: 15.2 us -> 12.3 us  [body(): pl.pallas_call(functools.partial(finish_kernel, blocks, heads), out_shape...]
    convert_element_type x1 -> x0, other arithmetic: 2.03 us -> none  [body(): normed = row_norm(tokens.astype(F32), input_gain).astype(BF16)]
    unnamed x9 -> x5, local copies, waits for them, and re-layouts: 3.36 us -> 4.04 us
  transfers between devices with their start and end apart: 2 -> 0, of which waited for: 0 -> 0; matrix products, arithmetic and copies ran while one was open for 1% -> 0% of each run, Pallas kernels for 60% -> 0%
where the time goes in v2:
time: 127 us; the launch traced here: 124 us
  Pallas kernels  118 us (93%)
  local copies, waits for them, and re-layouts  5.28 us (4%)
    pallas_call x1, Pallas kernels, body(): pl.pallas_call(functools.partial(recur_kernel, blocks, heads), out_shape=...  35.4 us
    pallas_call x1, Pallas kernels, body(): pl.pallas_call(functools.partial(attend_kernel, blocks, heads, pair ** (-...  32.9 us
    pallas_call x1, Pallas kernels, body(): pl.pallas_call(functools.partial(project_kernel, widths, heads), out_shap...  23.6 us
    pallas_call x1, Pallas kernels, body(): pl.pallas_call(functools.partial(merge_kernel, groups), out_shape=shape((...  13.9 us
    pallas_call x1, Pallas kernels, body(): pl.pallas_call(functools.partial(finish_kernel, blocks, heads), out_shape...  12.3 us
    unnamed x5, local copies, waits for them, and re-layouts  4.04 us

profile of v2, /device:TPU:31, one launch (start us, length us, event | category | flops | bytes accessed | tf_op | source)
XLA Modules:
  0.0 124.1 jit_solution(8062578613542122143)
XLA Ops:
  0.6 1.2 %dynamic_slice.3 = f32[1]{0:T(128)} dynamic-slice(f32[4]{0:T(128)} %param.34, s32[]{:T(128)S(6)} %select_n.9), dynamic_slice_sizes={1} | dynamic-slice | bytes 12 | tf_op jit(solution)/shard_map/dynamic_slice | solution.py:603
  1.9 1.5 %copy.21 = f32[4,512]{0,1:T(8,128)} copy(f32[4,512]{1,0:T(4,128)} %param.31) | data formatting | bytes 16384 | tf_op args[12]
  3.4 23.6 %project.1 = (bf16[512,512]{1,0:T(8,128)(2,1)}, bf16[512,512]{1,0:T(8,128)(2,1)}, bf16[512,256]{1,0:T(8,128)(2,1)}, bf16[512,256]{1,0:T(8,128)(2,1)}, bf16[4,512...) custom-call(bf16[128,2048]{1,0:T(8,128)(2,1)} %refs_0_.2, f32[1,2048]{1,0:T(1,128)} %bitcast.8, ...), custom_call_target="tpu_custom_call" | custom-call | tf_op jit(solution)/shard_map/project/pallas_call | solution.py:546
  27.1 35.4 %recur.1 = (f32[512,256]{1,0:T(8,128)}, bf16[512,512]{1,0:T(8,128)(2,1)}, bf16[4,64,128]{2,1,0:T(8,128)(2,1)}, f32[8,512]{1,0:T(8,128)}, bf16[8,512,128]{2,1,0:T...) custom-call(bf16[512,512]{1,0:T(8,128)(2,1)} %get-tuple-element.25.rq, ...), custom_call_target="tpu_custom_call" | custom-call | tf_op jit(solution)/shard_map/recur/pallas_call | solution.py:571
  62.4 32.9 %attend.1 = (bf16[8,128,128]{2,1,0:T(8,128)(2,1)}, f32[8,8,256]{2,1,0:T(8,128)}, f32[4,64,128]{2,1,0:T(8,128)}, bf16[256,2048]{1,0:T(8,128)(2,1)}, bf16[256,2048...) custom-call(bf16[8,128,128]{2,1,0:T(8,128)(2,1)} %get-tuple-element.30.q_all, ...), custom_call_target="tpu_custom_call" | custom-call | tf_op jit(solution)/shard_map/attend/pallas_call | solution.py:604
  95.4 12.3 %finish.1 = (bf16[512,512]{1,0:T(8,128)(2,1)}, f32[2,4,512]{2,1,0:T(4,128)}, bf16[256,2048]{1,0:T(8,128)(2,1)}) custom-call(bf16[8,128,128]{2,1,0:T(8,128)(2,1)} %get-tuple-element.35.msg, f32[8,8,256]{2,1,0:T(8,128)} %get-tuple-element.36.lmsg, f32[512,256]{1,0:T(8,128)} %get-tuple-element.37.local, bf16[512,512]{1,0:T(8,128)(2,1)} %get-tuple-element.38.qdecay, ...), custom_call_target="tpu_custom_call" | custom-call | tf_op jit(solution)/shard_map/finish/pallas_call | solution.py:638
  107.7 0.0 copy-start
  107.7 13.9 %merge.1 = bf16[128,2048]{1,0:T(8,128)(2,1)} custom-call(bf16[512,512]{1,0:T(8,128)(2,1)} %get-tuple-element.42.mixed, f32[1,2048]{1,0:T(1,128)} %bitcast.9, bf16[256,2048]{1,0:T(8,128)(2,1)} %refs_0_.3, bf16[256,2048]{1,0:T(8,128)(2,1)} %get-tuple-element.34.far_r.refs_1_, bf16[256,2048]{1,0:T(8,128)(2,1)} %get-tuple-element.43.refs_2_, ...), custom_call_target="tpu_custom_call" | custom-call | tf_op jit(solution)/shard_map/merge/pallas_call | solution.py:659
  121.6 1.9 %copy.24 = bf16[128,2048]{1,0:T(8,128)(2,1)} copy(bf16[128,2048]{1,0:T(8,128)(2,1)} %merge.1) | data formatting | bytes 1048576
  123.5 0.0 copy-done
  123.5 0.6 copy.25
Async XLA Ops:
  107.7 15.8 %copy-start = (f32[2,4,512]{2,1,0:T(4,128)S(1)}, f32[2,4,512]{2,1,0:T(4,128)}, u32[]{:S(2)}) copy-start(f32[2,4,512]{2,1,0:T(4,128)} %get-tuple-element.51) | copy-start | bytes 49156

commit v3 on v2

--- a/solution.py
+++ b/solution.py
@@ -187,24 +187,35 @@
 
 
 def recur_kernel(n, heads, rq, rf, ri, kv, qs, floor, shift, own_r, *refs):
-    local, qdecay, state, total, kv_all, q_all, far_r, st, ssem, rsem, lsem, xsem = refs
+    local, qdecay, state, total, kv_all, q_all, far_r = refs[:7]
+    st, turned, ssem, rsem, fsem, gsem, lsem, xsem = refs[7:]
     _, far, _, _ = around()
     me = lax.axis_index("sp")
     share = n // heads
     rows = rq.shape[0]
     keys = floor.shape[1] // heads
     width = ri.shape[1] // heads
+    head, portion = me // share, lax.rem(me, share)
     meet("sp", n, far)
+    direct = []
+    for k in range(1, heads):
+        other = lax.rem(head + k, heads)
+        direct.append(
+            remote(
+                kv.at[other],
+                kv_all.at[me],
+                ssem.at[0, k],
+                rsem.at[0, k],
+                "sp",
+                other * share + portion,
+            )
+        )
     copies = []
     for k in range(1, n):
         peer = lax.rem(me + k, n)
-        head, portion = peer // share, lax.rem(peer, share)
-        copies.append(
-            remote(kv.at[head], kv_all.at[me], ssem.at[0, k], rsem.at[0, k], "sp", peer)
-        )
         copies.append(
             remote(
-                qs.at[head, portion],
+                qs.at[peer // share, lax.rem(peer, share)],
                 q_all.at[me],
                 ssem.at[1, k],
                 rsem.at[1, k],
@@ -212,14 +223,37 @@
                 peer,
             )
         )
+
+    def forward(k):
+        source = lax.rem(head + heads - k, heads) * share + portion
+        block = kv.at[head] if k == 0 else kv_all.at[source]
+        return [
+            remote(
+                block,
+                kv_all.at[source],
+                fsem.at[k, j],
+                gsem.at[k, j],
+                "sp",
+                head * share + lax.rem(portion + j, share),
+            )
+            for j in range(1, share)
+        ]
+
+    for cp in direct:
+        cp.start()
+    forwards = forward(0)
+    for cp in forwards:
+        cp.start()
     copies.append(remote(own_r, far_r, xsem.at[0], xsem.at[1], "tp", far))
     for cp in copies:
         cp.start()
-    head, portion = me // share, lax.rem(me, share)
     own_kv = pltpu.make_async_copy(kv.at[head], kv_all.at[me], lsem.at[0])
     own_q = pltpu.make_async_copy(qs.at[head, portion], q_all.at[me], lsem.at[1])
     own_kv.start()
     own_q.start()
+    turned[...] = jnp.transpose(
+        jnp.concatenate([shift[...], jnp.zeros((128 - heads, rows), F32)], axis=0)
+    )
 
     st[...] = jnp.zeros_like(st)
     lower = lax.broadcasted_iota(jnp.int32, (SPAN, SPAN), 0) >= lax.broadcasted_iota(
@@ -230,7 +264,7 @@
     def chunk(i, run):
         at = pl.ds(pl.multiple_of(i * SPAN, SPAN), SPAN)
         key = floor[...] * jax.nn.sigmoid(-rf[at, :].astype(F32))
-        moves = shift[at, :]
+        moves = turned[at, :]
         decay = jnp.log1p(-key) + jnp.concatenate(
             [jnp.broadcast_to(moves[:, h : h + 1], (SPAN, keys)) for h in range(heads)], axis=1
         )
@@ -260,8 +294,17 @@
     run = lax.fori_loop(0, rows // SPAN, chunk, jnp.zeros((1, heads * keys), F32))
     state[...] = st[...].astype(BF16)
     total[...] = jnp.broadcast_to(run, total.shape)
+    for k in range(1, heads):
+        direct[k - 1].wait_recv()
+        for cp in forward(k):
+            cp.start()
     own_kv.wait()
     own_q.wait()
+    for cp in direct:
+        cp.wait_send()
+    for k in range(heads):
+        for cp in forward(k):
+            cp.wait()
     for cp in copies:
         cp.wait()
 
@@ -362,7 +405,7 @@
 
         acc1, acc2 = lax.fori_loop(0, b + 1, weigh, (jnp.zeros((mine, 2 * width), F32),) * 2)
         sum1, sum2 = acc1[:, width : width + 1], acc2[:, width : width + 1]
-        out = acc1[:, :width] / sum1 - lam[0, 0] * (acc2[:, :width] / sum2)
+        out = acc1[:, :width] / sum1 - lam[me // share] * (acc2[:, :width] / sum2)
         out = row_norm(out, gain[...]).astype(BF16)
         msg[b] = jnp.concatenate([out[: mine // 2], out[mine // 2 :]], axis=1)
         log1 = (tops[0] + jnp.log2(sum1)) * math.log(2.0)
@@ -583,8 +626,11 @@
         out_specs=(VMEM,) * 6 + (ANY,),
         scratch_shapes=[
             pltpu.VMEM((heads, width, keys), F32),
+            pltpu.VMEM((rows, 128), F32),
             dma((2, blocks)),
             dma((2, blocks)),
+            dma((heads, share)),
+            dma((heads, share)),
             dma((2,)),
             dma((2,)),
         ],
@@ -597,10 +643,9 @@
         kv,
         qs,
         forget_floor.reshape(1, heads * keys),
-        jnp.transpose(decay_shift),
+        decay_shift,
         recur_out,
     )
-    lam = lax.dynamic_slice_in_dim(diff_lambda, lax.axis_index("sp") // share, 1, 0)
     msg, lmsg, incoming, sib_r, diag_r, far_d, sib_d = pl.pallas_call(
         functools.partial(attend_kernel, blocks, heads, pair ** (-0.5) / math.log(2.0)),
         out_shape=(
@@ -629,7 +674,7 @@
         kv_all,
         state,
         total,
-        lam.reshape(1, 1),
+        diff_lambda,
         diff_gain.reshape(1, width),
         recur_out,
         far_r,

time: 127 us -> 117 us (0.921); the launches traced: 124 us -> 115 us
  Pallas kernels: 118 us -> 112 us
  local copies, waits for them, and re-layouts: 5.28 us -> 2.49 us
    pallas_call x1, Pallas kernels: 35.4 us -> 28.3 us  [body(): pl.pallas_call(functools.partial(recur_kernel, blocks, heads), out_shape=...]
    unnamed x5 -> x4, local copies, waits for them, and re-layouts: 4.04 us -> 2.49 us
    pallas_call x1, Pallas kernels: 32.9 us -> 34.3 us  [body(): pl.pallas_call(functools.partial(attend_kernel, blocks, heads, pair ** (-...]
where the time goes in v3:
time: 117 us; the launch traced here: 115 us
  Pallas kernels  112 us (96%)
  local copies, waits for them, and re-layouts  2.49 us (2%)
    pallas_call x1, Pallas kernels, body(): pl.pallas_call(functools.partial(attend_kernel, blocks, heads, pair ** (-...  34.3 us
    pallas_call x1, Pallas kernels, body(): pl.pallas_call(functools.partial(recur_kernel, blocks, heads), out_shape=...  28.3 us
    pallas_call x1, Pallas kernels, body(): pl.pallas_call(functools.partial(project_kernel, widths, heads), out_shap...  23.6 us
    pallas_call x1, Pallas kernels, body(): pl.pallas_call(functools.partial(merge_kernel, groups), out_shape=shape((...  14.7 us
    pallas_call x1, Pallas kernels, body(): pl.pallas_call(functools.partial(finish_kernel, blocks, heads), out_shape...  11.4 us
    unnamed x4, local copies, waits for them, and re-layouts  2.49 us

profile of v3, /device:TPU:31, one launch (start us, length us, event | category | flops | bytes accessed | tf_op | source)
XLA Modules:
  0.0 115.5 jit_solution(18198306937376964775)
XLA Ops:
  0.6 23.6 %project.1 = (bf16[512,512]{1,0:T(8,128)(2,1)}, bf16[512,512]{1,0:T(8,128)(2,1)}, bf16[512,256]{1,0:T(8,128)(2,1)}, bf16[512,256]{1,0:T(8,128)(2,1)}, bf16[4,512...) custom-call(bf16[128,2048]{1,0:T(8,128)(2,1)} %refs_0_.2, f32[1,2048]{1,0:T(1,128)} %bitcast.5, ...), custom_call_target="tpu_custom_call" | custom-call | tf_op jit(solution)/shard_map/project/pallas_call | solution.py:589
  24.3 28.3 %recur.1 = (f32[512,256]{1,0:T(8,128)}, bf16[512,512]{1,0:T(8,128)(2,1)}, bf16[4,64,128]{2,1,0:T(8,128)(2,1)}, f32[8,512]{1,0:T(8,128)}, bf16[8,512,128]{2,1,0:T...) custom-call(bf16[512,512]{1,0:T(8,128)(2,1)} %get-tuple-element.25.rq, ...), custom_call_target="tpu_custom_call" | custom-call | tf_op jit(solution)/shard_map/recur/pallas_call | solution.py:614
  52.6 34.3 %attend.1 = (bf16[8,128,128]{2,1,0:T(8,128)(2,1)}, f32[8,8,256]{2,1,0:T(8,128)}, f32[4,64,128]{2,1,0:T(8,128)}, bf16[256,2048]{1,0:T(8,128)(2,1)}, bf16[256,2048...) custom-call(bf16[8,128,128]{2,1,0:T(8,128)(2,1)} %get-tuple-element.30.q_all, ...), custom_call_target="tpu_custom_call" | custom-call | tf_op jit(solution)/shard_map/attend/pallas_call | solution.py:649
  86.9 11.4 %finish.1 = (bf16[512,512]{1,0:T(8,128)(2,1)}, f32[2,4,512]{2,1,0:T(4,128)}, bf16[256,2048]{1,0:T(8,128)(2,1)}) custom-call(bf16[8,128,128]{2,1,0:T(8,128)(2,1)} %get-tuple-element.35.msg, f32[8,8,256]{2,1,0:T(8,128)} %get-tuple-element.36.lmsg, f32[512,256]{1,0:T(8,128)} %get-tuple-element.37.local, bf16[512,512]{1,0:T(8,128)(2,1)} %get-tuple-element.38.qdecay, ...), custom_call_target="tpu_custom_call" | custom-call | tf_op jit(solution)/shard_map/finish/pallas_call | solution.py:683
  98.3 0.0 copy-start
  98.3 14.7 %merge.1 = bf16[128,2048]{1,0:T(8,128)(2,1)} custom-call(bf16[512,512]{1,0:T(8,128)(2,1)} %get-tuple-element.42.mixed, f32[1,2048]{1,0:T(1,128)} %bitcast.6, bf16[256,2048]{1,0:T(8,128)(2,1)} %refs_0_.3, bf16[256,2048]{1,0:T(8,128)(2,1)} %get-tuple-element.34.far_r.refs_1_, bf16[256,2048]{1,0:T(8,128)(2,1)} %get-tuple-element.43.refs_2_, ...), custom_call_target="tpu_custom_call" | custom-call | tf_op jit(solution)/shard_map/merge/pallas_call | solution.py:704
  113.0 1.9 %copy.23 = bf16[128,2048]{1,0:T(8,128)(2,1)} copy(bf16[128,2048]{1,0:T(8,128)(2,1)} %merge.1) | data formatting | bytes 1048576
  114.9 0.0 copy-done
  114.9 0.6 copy.24
Async XLA Ops:
  98.3 16.6 %copy-start = (f32[2,4,512]{2,1,0:T(4,128)S(1)}, f32[2,4,512]{2,1,0:T(4,128)}, u32[]{:S(2)}) copy-start(f32[2,4,512]{2,1,0:T(4,128)} %get-tuple-element.51) | copy-start | bytes 49156
